TPU v7x, 512 devices: a whole 4x8x8 slice. The times are simulated.
512 devices in a mesh: sp: 64 (over z, y), fs: 4 (over x), tp: 2 (over core).
Axes of the slice: x: 4, y: 8, z: 8, core: 2. Of those that a mesh axis runs over, the one named last changes fastest.
Arguments:
- tokens: bfloat16 [16384, 2048], P('sp'), may hold values from -6 to 6
- norm_gain: float32 [2048], replicated, may hold values from 0.1 to 1.9
- conv_value: bfloat16 [2048, 1024], P('sp', ('fs', 'tp')), may hold values from -0.125 to 0.125
- conv_gate: bfloat16 [2048, 1024], P('sp', ('fs', 'tp')), may hold values from -0.125 to 0.125
- mixer_gate: bfloat16 [2048, 1024], P('sp', ('fs', 'tp')), may hold values from -0.125 to 0.125
- state_input: bfloat16 [2048, 1024], P('sp', ('fs', 'tp')), may hold values from -0.125 to 0.125
- write_projection: bfloat16 [2048, 1024], P('sp', ('fs', 'tp')), may hold values from -0.125 to 0.125
- state_read: bfloat16 [2048, 1024], P('sp', ('fs', 'tp')), may hold values from -0.125 to 0.125
- step_proj: bfloat16 [2048, 16], replicated, may hold values from -0.125 to 0.125
- step_bias: float32 [16], P(('fs', 'tp')), may hold values from -6 to -0.5
- decay_log: float32 [16], P(('fs', 'tp')), may hold values from -9 to -1.5
- decay_extra: float32 [16, 16384], P(('fs', 'tp'), 'sp'), may hold values from -0.8 to 0
- input_taps: float32 [4, 1024], P(None, ('fs', 'tp')), may hold values from -3 to 3
- write_taps: float32 [4, 1024], P(None, ('fs', 'tp')), may hold values from -3 to 3
- fetch_kernel_coefficients: float32 [4, 1024], P(None, ('fs', 'tp')), may hold values from -3 to 3
- long_taps: float32 [31, 1024], P(None, ('fs', 'tp')), may hold values from -5 to 5
- conv_gain: float32 [1024], P(('fs', 'tp')), may hold values from 0.1 to 1.9
- state_gain: float32 [1024], P(('fs', 'tp')), may hold values from 0.1 to 1.9
- conv_output: bfloat16 [2048, 1024], P('sp', ('fs', 'tp')), may hold values from -0.125 to 0.125
- state_output: bfloat16 [2048, 1024], P('sp', ('fs', 'tp')), may hold values from -0.125 to 0.125
- initial_state: float32 [16, 64, 128], P(('fs', 'tp')), may hold values from -12 to 12
Outputs:
- mixed: bfloat16 [16384, 2048], P(('sp', 'fs', 'tp'))
All inputs are finite; a program needn't handle non-finite values.
Results may differ from a plain program's by a relative error of at most 0.017.
Values may be sent and summed in bfloat16 or wider, within the bound.
No kernel may reach another device: no remote copies, remote signals or barrier semaphores. Data moves between devices by JAX's collectives and lax.ppermute only.
A program may use at most 64 MiB of HBM per device.

v0:
```python
import jax
import jax.numpy as jnp
from jax import lax
from jax.sharding import Mesh
from jax.sharding import PartitionSpec as P

C_CH = 1024
STATE = 128
WIDE_TAPS = 31
SHORT_TAPS = 4
SPAN = 64
D_INNER = 1024
SP = ("sp_0", "sp_1")
SP_FS_TP = ("sp_0", "sp_1", "fs", "tp")


eps_norm = 1e-06


def sent_together(arrays, axis, dim, along):
    both = jnp.concatenate(arrays, axis=along)
    out, at, finished = (lax.all_gather(both, axis, axis=dim, tiled=True), 0, [])
    for a in arrays:
        finished.append(lax.slice_in_dim(out, at, at + a.shape[along], axis=along))
        at += a.shape[along]
    return tuple(finished)


def shifted(block, axis, distance):
    devices = range(lax.axis_size(axis))
    route = [(i - distance, i) for i in devices if i - distance in devices]
    return lax.ppermute(block, axis, route)


def sent_to_all(shard, axis):
    size = lax.axis_size(axis)
    return lax.all_to_all(
        jnp.broadcast_to(shard[None], (size, *shard.shape)), axis, 0, 0, tiled=True
    )


def over_copies(shard, axis):
    everything = sent_to_all(shard, axis)
    return jnp.sum(everything, axis=0)


def nothing_yet(shard, identity):
    return jax.tree.map(
        lambda a, e: jnp.broadcast_to(jnp.asarray(e, a.dtype), a.shape), shard, identity
    )


def collected_together(shard, axis):
    leaves = jax.tree.leaves(shard)
    order = sorted(range(len(leaves)), key=lambda k: -leaves[k].size)
    width = (1, *leaves[order[0]].shape)[-1]
    lines = [
        jnp.pad(leaves[k].reshape(-1), (0, -leaves[k].size % width)).reshape(-1, width)
        for k in order
    ]
    both, at, found = (lax.all_gather(jnp.concatenate(lines), axis), 0, {})
    for k, line in zip(order, lines):
        piece = both[:, at : at + len(line)].reshape(len(both), -1)
        found[k] = piece[:, : leaves[k].size].reshape(-1, *leaves[k].shape)
        at += len(line)
    numbers = iter(range(len(leaves)))
    return jax.tree.map(lambda _: found[next(numbers)], shard)


def entering_2(shard, axes, combine, identity):
    before = start = nothing_yet(shard, identity)
    subtotal = shard
    for axis in reversed(axes):
        size, index = (lax.axis_size(axis), lax.axis_index(axis))
        pieces = collected_together(
            jax.tree.map(
                lambda part, kind: part.astype(kind), subtotal, (jnp.bfloat16, jnp.bfloat16)
            ),
            axis,
        )
        inside, subtotal = (start, start)
        for k in range(size):
            passed = k < index
            subtotal = combine(
                subtotal, jax.tree.map(lambda part, own: part[k].astype(own.dtype), pieces, shard)
            )
            inside = jax.tree.map(lambda new, old: jnp.where(passed, new, old), subtotal, inside)
        before = combine(inside, before)
    return before


def cut_along(shard, dim, size):
    before, after = (shard.shape[:dim], shard.shape[dim + 1 :])
    return jnp.moveaxis(shard.reshape(*before, size, -1, *after), dim, 0)


def summed_on_arrival(shard, axis, dim):
    size = lax.axis_size(axis)
    pieces = lax.all_to_all(cut_along(shard, dim, size), axis, 0, 0, tiled=True)
    return jnp.sum(pieces.astype(jnp.float32), axis=0)


def causal_valid(padded, taps):
    result = lax.conv_general_dilated(
        padded[None],
        taps[:, None, :],
        window_strides=(1,),
        padding="VALID",
        dimension_numbers=("NWC", "WIO", "NWC"),
        feature_group_count=taps.shape[1],
    )
    return result[0]


def project(normed, weight):
    return jnp.dot(normed, weight, preferred_element_type=jnp.float32).astype(jnp.bfloat16)


def carry_step(state, inputs):
    fresh, last = inputs
    return (state * jnp.exp(last)[:, None, None] + fresh, state)


def combine_states(earlier, later):
    return (earlier[0] + later[0], jnp.exp(later[0])[:, None, None] * earlier[1] + later[1])


def per_device(
    tokens,
    norm_gain,
    conv_value,
    conv_gate,
    mixer_gate,
    state_input,
    write_projection,
    state_read,
    step_proj,
    step_bias,
    decay_log,
    decay_extra,
    input_taps,
    write_taps,
    fetch_kernel_coefficients,
    long_taps,
    conv_gain,
    state_gain,
    conv_output,
    state_output,
    initial_state,
):
    rows = tokens.shape[0]
    channels = conv_value.shape[1]
    width_in = state_input.shape[1]
    width_group = write_projection.shape[1]
    heads = step_bias.shape[0]
    groups = width_group // STATE
    per_group = heads // groups
    head_size = width_in // heads
    values = tokens.astype(jnp.float32)
    normed = (
        values * lax.rsqrt(jnp.mean(values * values, axis=1, keepdims=True) + eps_norm) * norm_gain
    ).astype(jnp.bfloat16)
    (
        whole_value,
        whole_gate,
        whole_input,
        whole_write,
        whole_read,
        whole_mixer,
        back_conv,
        back_state,
    ) = sent_together(
        (
            conv_value,
            conv_gate,
            state_input,
            write_projection,
            state_read,
            mixer_gate,
            conv_output,
            state_output,
        ),
        SP,
        0,
        1,
    )
    input_rows = project(normed, whole_input)
    write_rows = project(normed, whole_write)
    read_rows = project(normed, whole_read)
    gate_z = project(normed, whole_mixer)
    value_rows = project(normed, whole_value)
    gate_rows = project(normed, whole_gate)
    step_all = jnp.dot(normed, step_proj, preferred_element_type=jnp.float32)
    head_start = (lax.axis_index("fs") * lax.axis_size("tp") + lax.axis_index("tp")) * heads
    step_raw = lax.dynamic_slice_in_dim(step_all, head_start, heads, 1)
    step_size = jax.nn.softplus(step_raw + step_bias)
    log_step = -jnp.exp(decay_log) * step_size + decay_extra.T
    edge_width = WIDE_TAPS - 1
    tail = rows - edge_width
    packed = jnp.concatenate(
        [
            value_rows[tail:],
            gate_rows[tail:],
            input_rows[tail:],
            write_rows[tail:],
            read_rows[tail:],
        ],
        axis=1,
    )
    before = shifted(packed, SP, 1)
    short_edge = before[edge_width - SHORT_TAPS + 1 :, 2 * channels :]
    state_row_values = jnp.concatenate([input_rows, write_rows, read_rows], axis=1)
    state_full = jnp.concatenate([short_edge, state_row_values], axis=0).astype(jnp.float32)
    state_taps = jnp.concatenate([input_taps, write_taps, fetch_kernel_coefficients], axis=1)
    activated = jax.nn.silu(causal_valid(state_full, state_taps))
    input_act = activated[:, :width_in]
    write_activation = activated[:, width_in : width_in + width_group]
    read_act = activated[:, width_in + width_group :]
    blocks = rows // SPAN
    x_heads = (input_act.reshape(rows, heads, head_size) * step_size[:, :, None]).reshape(
        blocks, SPAN, heads, head_size
    )
    write_heads = jnp.repeat(
        write_activation.reshape(rows, groups, STATE), per_group, axis=1
    ).reshape(blocks, SPAN, heads, STATE)
    read_heads = jnp.repeat(read_act.reshape(rows, groups, STATE), per_group, axis=1).reshape(
        blocks, SPAN, heads, STATE
    )
    log_blocks = log_step.reshape(blocks, SPAN, heads)
    cumul = jnp.cumsum(log_blocks, axis=1)
    lower = jnp.tril(jnp.ones((SPAN, SPAN), dtype=bool))
    by_head = jnp.swapaxes(cumul, 1, 2)
    gaps = by_head[:, :, :, None] - by_head[:, :, None, :]
    weights = jnp.where(lower, jnp.exp(jnp.where(lower, gaps, 0.0)), 0.0)
    scores = jnp.einsum("bthn,bshn->bhts", read_heads, write_heads)
    inner = jnp.einsum("bhts,bshp->bthp", scores * weights, x_heads)
    last = cumul[:, -1]
    fresh = jnp.einsum(
        "bshn,bshp->bhpn", write_heads * jnp.exp(last[:, None, :] - cumul)[:, :, :, None], x_heads
    )
    state_end, block_states = lax.scan(
        carry_step, jnp.zeros((heads, head_size, STATE), jnp.float32), (fresh, last)
    )
    logsum = jnp.sum(last, axis=0)
    block_prefix = jnp.cumsum(last, axis=0) - last
    start_decay = jnp.exp(block_prefix[:, None, :] + cumul)
    local_out = (
        inner
        + jnp.einsum("bthn,bhpn->bthp", read_heads, block_states) * jnp.exp(cumul)[:, :, :, None]
    )
    value_full = jnp.concatenate([before[:, :channels], value_rows], axis=0).astype(jnp.float32)
    gate_full = jnp.concatenate([before[:, channels : 2 * channels], gate_rows], axis=0).astype(
        jnp.float32
    )
    glu = value_full * jax.nn.sigmoid(gate_full)
    long_mix = causal_valid(glu, long_taps)
    total_sum, total_square = (
        over_copies(jnp.sum(long_mix, axis=1), ("fs", "tp")),
        over_copies(jnp.sum(long_mix * long_mix, axis=1), ("fs", "tp")),
    )
    mean = total_sum / C_CH
    spread = total_square / C_CH - mean * mean
    conv_out = jax.nn.silu(
        (long_mix - mean[:, None]) * lax.rsqrt(spread + eps_norm)[:, None] * conv_gain
    ).astype(jnp.bfloat16)
    prefix_log, entering = entering_2(
        (logsum, state_end), SP, combine_states, (jnp.zeros_like(logsum), jnp.zeros_like(state_end))
    )
    start_state = entering + jnp.exp(prefix_log)[:, None, None] * initial_state
    outputs = (
        local_out
        + jnp.einsum("bthn,hpn->bthp", read_heads, start_state) * start_decay[:, :, :, None]
    )
    gated = outputs.reshape(rows, width_in) * jax.nn.silu(gate_z.astype(jnp.float32))
    quadratic_total = over_copies(jnp.sum(gated * gated, axis=1), ("fs", "tp"))
    state_out = (
        gated * lax.rsqrt(quadratic_total / D_INNER + eps_norm)[:, None] * state_gain
    ).astype(jnp.bfloat16)
    contract = (((1,), (1,)), ((), ()))
    out_rows = rows // (lax.axis_size("fs") * lax.axis_size("tp"))
    conv_part = lax.slice_in_dim(conv_out, 0, out_rows * lax.axis_size(("fs", "tp")), axis=0)
    term = lax.dot_general(conv_part, back_conv, contract, preferred_element_type=jnp.float32)
    mixed = summed_on_arrival(
        (
            term
            + lax.dot_general(state_out, back_state, contract, preferred_element_type=jnp.float32)
        ).astype(jnp.bfloat16),
        ("fs", "tp"),
        0,
    )
    return mixed.astype(jnp.bfloat16)


def solution(mesh):
    torus = Mesh(
        mesh.devices.reshape(8, 8, mesh.shape["fs"], mesh.shape["tp"]), ("sp_0", "sp_1", "fs", "tp")
    )
    in_specs = (
        P(SP, None),
        P(),
        P(SP, ("fs", "tp")),
        P(SP, ("fs", "tp")),
        P(SP, ("fs", "tp")),
        P(SP, ("fs", "tp")),
        P(SP, ("fs", "tp")),
        P(SP, ("fs", "tp")),
        P(),
        P(("fs", "tp")),
        P(("fs", "tp")),
        P(("fs", "tp"), SP),
        P(None, ("fs", "tp")),
        P(None, ("fs", "tp")),
        P(None, ("fs", "tp")),
        P(None, ("fs", "tp")),
        P(("fs", "tp")),
        P(("fs", "tp")),
        P(SP, ("fs", "tp")),
        P(SP, ("fs", "tp")),
        P(("fs", "tp"), None, None),
    )
    out_specs = P(SP_FS_TP, None)
    return jax.shard_map(
        per_device, mesh=torus, in_specs=in_specs, out_specs=out_specs, check_vma=False
    )
```

profile of v0, /device:TPU:1, one launch (start us, length us, event | category | flops | bytes accessed | tf_op | source)
XLA Modules:
  0.0 235.7 jit_solution(578566535411008328)
XLA Ops:
  6.6 0.7 constant_dynamic-update-slice_fusion.7
  7.3 0.7 constant_dynamic-update-slice_fusion.6
  8.0 0.7 constant_dynamic-update-slice_fusion.5
  8.8 0.8 constant_dynamic-update-slice_fusion.4
  9.5 0.7 constant_dynamic-update-slice_fusion.3
  10.3 0.7 constant_dynamic-update-slice_fusion.2
  11.0 0.7 constant_dynamic-update-slice_fusion.1
  11.7 0.7 constant_dynamic-update-slice_fusion
  12.4 0.6 copy-done.2
  13.0 1.5 fusion.3
  14.5 0.7 exponential_negate_fusion
  15.2 1.7 fusion.164
  17.6 83.7 %all-gather.6.cloned.1.call-done = bf16[2048,1024]{1,0:T(8,128)(2,1)} async-done(((bf16[32,1024]{1,0:T(8,128)(2,1)}), bf16[2048,1024]{1,0:T(8,128)(2,1)}) %all-gather.6.cloned.1.call-update) | async-done | bytes 4194320 | tf_op jit(solution)/shard_map/all_gather | solution.py:22
  101.3 1.5 convolution_convert_fusion.5
  102.9 1.5 convolution_convert_fusion.4
  104.4 1.5 convolution_convert_fusion.3
  106.0 1.5 convolution_convert_fusion.2
  107.6 1.5 convolution_convert_fusion.1
  109.1 2.8 %collective-permute-start = (bf16[30,640]{1,0:T(8,128)(2,1)S(1)}, bf16[30,640]{1,0:T(8,128)(2,1)S(1)}, u32[]{:S(2)}, u32[]{:S(2)}) collective-permute-start(bf16[30,640]{1,0:T(8,128)(2,1)S(1)} %constant_dynamic-update-slice_fusion.8), channel_id=1, source_target_pairs={{0,8},{8,16},{16,24},{24,32},{32,40},{40,48},{48,56},{56,64},{64,7... | collective-permute-start | bytes 115208 | tf_op jit(solution)/shard_map/ppermute | solution.py:32
  112.1 0.1 copy.181
  112.6 0.4 collective-permute-done
  113.8 0.2 reshape.537
  114.0 0.3 broadcast_multiply_fusion
  114.4 0.3 fusion.25
  114.7 0.5 while.13
  115.3 20.1 %all-gather.2 = bf16[8,129,128]{2,1,0:T(8,128)(2,1)S(1)} all-gather(bf16[1,129,128]{2,1,0:T(8,128)(2,1)S(1)} %maximum_bitcast_fusion.1), channel_id=2, replica_groups=mesh['sp_0'=8,'sp_1'=8,'fs'=4,'tp'=2] {'sp_1'}, dimensions={0}, use_global_device_ids=true | all-gather | bytes 297216 | tf_op jit(solution)/shard_map/all_gather | solution.py:61
  136.6 0.2 fusion.72
  136.9 20.1 %all-gather.3 = bf16[8,129,128]{2,1,0:T(8,128)(2,1)S(1)} all-gather(bf16[1,129,128]{2,1,0:T(8,128)(2,1)S(1)} %maximum_bitcast_fusion.2), channel_id=3, replica_groups=mesh['sp_0'=8,'sp_1'=8,'fs'=4,'tp'=2] {'sp_0'}, dimensions={0}, use_global_device_ids=true | all-gather | bytes 297216 | tf_op jit(solution)/shard_map/all_gather | solution.py:61
  157.2 0.4 convolution_select_fusion.1
  157.6 0.3 convolution_bitcast_fusion.1
  158.0 0.2 fusion.7
  158.2 0.4 fusion.9
  158.6 0.2 copy.184
  158.8 0.2 reshape.647
  159.0 1.6 multiply_reduce_fusion
  160.6 0.6 broadcast_in_dim.53
  161.2 22.5 %all-to-all-start.2 = ((f32[8,1,256]{2,1,0:T(1,128)}), f32[8,1,256]{2,1,0:T(1,128)S(1)}, u32[]{:S(2)}, u32[]{:S(2)}) async-start(f32[8,1,256]{2,1,0:T(1,128)} %broadcast_in_dim.53), calls=%async_computation.2 | async-start | bytes 16384 | tf_op jit(solution)/shard_map/all_to_all | solution.py:37
  183.9 4.4 %all-to-all-done.2 = f32[8,1,256]{2,1,0:T(1,128)S(1)} async-done(((f32[8,1,256]{2,1,0:T(1,128)}), f32[8,1,256]{2,1,0:T(1,128)S(1)}, u32[]{:S(2)}, u32[]{:S(2)}) %all-to-all-start.2) | async-done | bytes 8224 | tf_op jit(solution)/shard_map/all_to_all | solution.py:37
  188.4 0.6 broadcast_in_dim.42
  189.0 3.9 %all-to-all-start = ((f32[8,1,256]{2,1,0:T(1,128)}), f32[8,1,256]{2,1,0:T(1,128)S(1)}, u32[]{:S(2)}, u32[]{:S(2)}) async-start(f32[8,1,256]{2,1,0:T(1,128)} %broadcast_in_dim.42), calls=%async_computation | async-start | bytes 16384 | tf_op jit(solution)/shard_map/all_to_all | solution.py:37
  193.0 4.6 %all-to-all-done = f32[8,1,256]{2,1,0:T(1,128)S(1)} async-done(((f32[8,1,256]{2,1,0:T(1,128)}), f32[8,1,256]{2,1,0:T(1,128)S(1)}, u32[]{:S(2)}, u32[]{:S(2)}) %all-to-all-start) | async-done | bytes 8224 | tf_op jit(solution)/shard_map/all_to_all | solution.py:37
  197.5 0.6 broadcast_in_dim.43
  198.1 3.9 %all-to-all-start.1 = ((f32[8,1,256]{2,1,0:T(1,128)}), f32[8,1,256]{2,1,0:T(1,128)S(1)}, u32[]{:S(2)}, u32[]{:S(2)}) async-start(f32[8,1,256]{2,1,0:T(1,128)} %broadcast_in_dim.43), calls=%async_computation.1 | async-start | bytes 16384 | tf_op jit(solution)/shard_map/all_to_all | solution.py:37
  202.1 4.6 %all-to-all-done.1 = f32[8,1,256]{2,1,0:T(1,128)S(1)} async-done(((f32[8,1,256]{2,1,0:T(1,128)}), f32[8,1,256]{2,1,0:T(1,128)S(1)}, u32[]{:S(2)}, u32[]{:S(2)}) %all-to-all-start.1) | async-done | bytes 8224 | tf_op jit(solution)/shard_map/all_to_all | solution.py:37
  206.8 1.6 fusion.13
  208.4 1.6 fusion.2
  210.0 18.0 %all_to_all.23 = bf16[8,32,2048]{2,1,0:T(8,128)(2,1)S(1)} all-to-all(bf16[8,32,2048]{2,1,0:T(8,128)(2,1)S(1)} %bitcast.202), channel_id=1, replica_groups=mesh['sp_0'=8,'sp_1'=8,'fs'=4,'tp'=2] {'fs','tp'}, dimensions={0} | all-to-all | bytes 2097152 | tf_op jit(solution)/shard_map/all_to_all | solution.py:99
  228.0 0.8 reduce_sum.92
  (125 shorter events, 4.4 us)
Async XLA Ops:
  6.5 8.7 %copy-start = (bf16[2048,16]{0,1:T(8,128)(2,1)S(1)}, bf16[2048,16]{0,1:T(8,128)(2,1)}, u32[]{:S(2)}) copy-start(bf16[2048,16]{0,1:T(8,128)(2,1)} %param.31) | copy-start | bytes 196612
  6.5 10.4 %copy-start.4 = (f32[2,256]{1,0:T(2,128)S(1)}, f32[2,256]{1,0:T(2,128)}, u32[]{:S(2)}) copy-start(f32[2,256]{1,0:T(2,128)} %param.34) | copy-start | bytes 6148
  6.5 10.4 %copy-start.9 = (f32[2]{0:T(128)S(1)}, f32[2]{0:T(128)}, u32[]{:S(2)}) copy-start(f32[2]{0:T(128)} %param.32) | copy-start | bytes 28
  6.5 11.0 %copy-start.5 = (f32[4,128]{1,0:T(4,128)S(1)}, f32[4,128]{1,0:T(4,128)}, u32[]{:S(2)}) copy-start(f32[4,128]{1,0:T(4,128)} %param.37) | copy-start | bytes 6148
  6.5 11.0 %copy-start.6 = (f32[4,128]{1,0:T(4,128)S(1)}, f32[4,128]{1,0:T(4,128)}, u32[]{:S(2)}) copy-start(f32[4,128]{1,0:T(4,128)} %param.36) | copy-start | bytes 6148
  6.5 11.0 %copy-start.7 = (f32[4,128]{1,0:T(4,128)S(1)}, f32[4,128]{1,0:T(4,128)}, u32[]{:S(2)}) copy-start(f32[4,128]{1,0:T(4,128)} %param.35) | copy-start | bytes 6148
  6.6 94.8 %all-gather.6.cloned.1.call-start = ((), (), s32[]{:S(2)}) async-start(), calls=%async_computation.4 | async-start | bytes 4259840 | tf_op jit(solution)/shard_map/all_gather | solution.py:22
  8.8 92.6 %copy-start.1 = (bf16[256,2048]{1,0:T(8,128)(2,1)S(1)}, bf16[256,2048]{1,0:T(8,128)(2,1)}, u32[]{:S(2)}) copy-start(bf16[256,2048]{1,0:T(8,128)(2,1)} %param.23) | copy-start | bytes 3145732
  8.8 92.6 %copy-start.12 = (f32[2048]{0:T(1024)S(1)}, f32[2048]{0:T(1024)}, u32[]{:S(2)}) copy-start(f32[2048]{0:T(1024)} %param.24) | copy-start | bytes 24580
  12.4 0.6 copy-start.2
  107.6 5.7 %copy-start.14 = (pred[8,33]{0,1:T(8,128)(4,1)S(1)}, pred[8,33]{0,1:T(8,128)(4,1)}, u32[]{:S(2)}) copy-start(pred[8,33]{0,1:T(8,128)(4,1)} %constant.111) | copy-start | bytes 796
  109.1 3.9 %collective-permute-start = (bf16[30,640]{1,0:T(8,128)(2,1)S(1)}, bf16[30,640]{1,0:T(8,128)(2,1)S(1)}, u32[]{:S(2)}, u32[]{:S(2)}) collective-permute-start(bf16[30,640]{1,0:T(8,128)(2,1)S(1)} %constant_dynamic-update-slice_fusion.8), channel_id=1, source_target_pairs={{0,8},{8,16},{16,24},{24,32},{32,40},{40,48},{48,56},{56,64},{64,7... | collective-permute-start | bytes 115208 | tf_op jit(solution)/shard_map/ppermute | solution.py:32
  115.2 42.0 %copy-start.11 = (f32[31,128]{1,0:T(8,128)S(1)}, f32[31,128]{1,0:T(8,128)}, u32[]{:S(2)}) copy-start(f32[31,128]{1,0:T(8,128)} %param.38) | copy-start | bytes 47620
  115.2 42.0 %copy-start.13 = (pred[8,36]{0,1:T(8,128)(4,1)S(1)}, pred[8,36]{0,1:T(8,128)(4,1)}, u32[]{:S(2)}) copy-start(pred[8,36]{0,1:T(8,128)(4,1)} %constant.110) | copy-start | bytes 868
  157.2 1.0 copy-start.3
  158.8 48.0 %copy-start.10 = (f32[128]{0:T(128)S(1)}, f32[128]{0:T(128)}, u32[]{:S(2)}) copy-start(f32[128]{0:T(128)} %param.39) | copy-start | bytes 1540
  160.6 47.7 %copy-start.8 = (f32[128]{0:T(128)S(1)}, f32[128]{0:T(128)}, u32[]{:S(2)}) copy-start(f32[128]{0:T(128)} %param.40) | copy-start | bytes 1540
  161.2 27.1 %all-to-all-start.2 = ((f32[8,1,256]{2,1,0:T(1,128)}), f32[8,1,256]{2,1,0:T(1,128)S(1)}, u32[]{:S(2)}, u32[]{:S(2)}) async-start(f32[8,1,256]{2,1,0:T(1,128)} %broadcast_in_dim.53), calls=%async_computation.2 | async-start | bytes 16384 | tf_op jit(solution)/shard_map/all_to_all | solution.py:37
  189.0 8.6 %all-to-all-start = ((f32[8,1,256]{2,1,0:T(1,128)}), f32[8,1,256]{2,1,0:T(1,128)S(1)}, u32[]{:S(2)}, u32[]{:S(2)}) async-start(f32[8,1,256]{2,1,0:T(1,128)} %broadcast_in_dim.42), calls=%async_computation | async-start | bytes 16384 | tf_op jit(solution)/shard_map/all_to_all | solution.py:37
  198.1 8.6 %all-to-all-start.1 = ((f32[8,1,256]{2,1,0:T(1,128)}), f32[8,1,256]{2,1,0:T(1,128)S(1)}, u32[]{:S(2)}, u32[]{:S(2)}) async-start(f32[8,1,256]{2,1,0:T(1,128)} %broadcast_in_dim.43), calls=%async_computation.1 | async-start | bytes 16384 | tf_op jit(solution)/shard_map/all_to_all | solution.py:37
Sparse Core Ops, SparseCore 0:
  13.1 88.1 all-gather.5
where the time goes:
time: 237 us; the launch traced here: 236 us
  waiting for transfers between devices  97.7 us (41%)
  blocking collectives  58.2 us (25%)
  starting transfers between devices  33.2 us (14%)
  matrix products  15.9 us (7%)
  between operations  14 us (6%)
  local copies, waits for them, and re-layouts  11.7 us (5%)
  other arithmetic  4.89 us (2%)
    all_gather x1, waiting for transfers between devices, sent_together(): lax.all_gather(both, axis, axis=dim, tiled=True)  83.7 us
    all_gather x2, blocking collectives, collected_together(): both, at, found = (lax.all_gather(jnp.concatenate(lines), axis), 0, {})  40.2 us
    all_to_all x3, starting transfers between devices, sent_to_all(): lax.all_to_all(jnp.broadcast_to(shard[None], (size, *shard.shape)), axis,...  30.4 us
    all_to_all x1, blocking collectives, summed_on_arrival(): pieces = lax.all_to_all(cut_along(shard, dim, size), axis, 0, 0, tiled=True)  18 us
    all_to_all x3, waiting for transfers between devices, sent_to_all(): lax.all_to_all(jnp.broadcast_to(shard[None], (size, *shard.shape)), axis,...  13.6 us
    dot_general x6, matrix products, project(): jnp.dot(normed, weight, preferred_element_type=jnp.float32)  9.35 us
    unnamed x45, local copies, waits for them, and re-layouts  6 us
  transfers between devices with their start and end apart: 5, of which 5 were waited for; matrix products, arithmetic and copies ran while one was open for 2% of the time, Pallas kernels for 0%

commit v1 on v0

v1 whole, which is shorter than its diff:
```python
import jax
import jax.numpy as jnp
from jax import lax
from jax.sharding import Mesh
from jax.sharding import PartitionSpec as P

C_CH = 1024
STATE = 128
D_INNER = 1024
WIDE = 31
SHORT = 4
HALO = 32
EPS = 1e-06
SP = ("sp_0", "sp_1")
FT = ("fs", "tp")
f32 = jnp.float32
bf16 = jnp.bfloat16


def spread(shard, axis):
    n = lax.axis_size(axis)
    return lax.all_to_all(jnp.broadcast_to(shard[None], (n, *shard.shape)), axis, 0, 0, tiled=True)


def previous(block):
    n = lax.axis_size(SP)
    return lax.ppermute(block, SP, [(i, i + 1) for i in range(n - 1)])


def dot(a, b, ca, cb):
    return lax.dot_general(a, b, (((ca,), (cb,)), ((), ())), preferred_element_type=f32)


def unit_rows(tokens, gain):
    v = tokens.astype(f32)
    return (v * lax.rsqrt(jnp.mean(v * v, axis=1, keepdims=True) + EPS) * gain).astype(bf16)


def causal(rows, taps, at, n):
    k = taps.shape[0]
    return sum(rows[at + i : at + i + n] * taps[i] for i in range(k))


def split3(x):
    hi = x.astype(bf16)
    rest = x - hi.astype(f32)
    mid = rest.astype(bf16)
    return hi, mid, (rest - mid.astype(f32)).astype(bf16)


def per_device(
    tokens, norm_gain, conv_value, conv_gate, mixer_gate, state_input, write_projection, state_read,
    step_proj, step_bias, decay_log, decay_extra, input_taps, write_taps, fetch_taps, long_taps,
    conv_gain, state_gain, conv_output, state_output, initial_state,
):
    rows = tokens.shape[0]
    ch = conv_value.shape[1]
    heads = step_bias.shape[0]
    p = ch // heads
    nf, nt = lax.axis_size("fs"), lax.axis_size("tp")
    shard = jnp.concatenate(
        [state_input, write_projection, state_read, mixer_gate, conv_value, conv_gate, conv_output, state_output], 1
    )
    near = spread(shard, "sp_1").reshape(-1, 8 * ch)
    rest = lax.all_gather(near[:, 2 * ch :], "sp_0", axis=0, tiled=True)
    first = spread(near[:, : 2 * ch], "sp_0").reshape(-1, 2 * ch)
    halo = previous(tokens[rows - HALO :])
    normed = unit_rows(jnp.concatenate([halo, tokens], 0), norm_gain)
    own = normed[HALO:]
    step_all = jnp.dot(own, step_proj, preferred_element_type=f32)
    me = lax.axis_index("fs") * nt + lax.axis_index("tp")
    step = jax.nn.softplus(lax.dynamic_slice_in_dim(step_all, me * heads, heads, 1) + step_bias)
    log_step = (-jnp.exp(decay_log) * step + decay_extra.T).T
    cumul = jnp.cumsum(log_step, axis=1)
    total = cumul[:, -1]
    xw = dot(normed, first, 1, 0).astype(bf16).astype(f32)
    x_act = jax.nn.silu(causal(xw[:, :ch], input_taps, HALO - SHORT + 1, rows))
    w_act = jax.nn.silu(causal(xw[:, ch:], write_taps, HALO - SHORT + 1, rows))
    xs = [(x_act[:, h * p : (h + 1) * p] * step[:, h : h + 1]).astype(bf16) for h in range(heads)]
    w16 = w_act.astype(bf16)
    left = jnp.exp(total[:, None] - cumul).T
    ends = jnp.concatenate(
        [dot(xs[h], (w_act * left[:, h : h + 1]).astype(bf16), 0, 0) for h in range(heads)], 0
    ).astype(bf16)
    hi, mid, lo = split3(total)
    logs = jnp.zeros((16, STATE), bf16)
    logs = logs.at[0, :heads].set(hi).at[1, :heads].set(mid).at[2, :heads].set(lo)
    got = spread(jnp.concatenate([ends, logs], 0), "sp_1")
    logs_y = jnp.sum(got[:, heads * p : heads * p + 3, :heads].astype(f32), 1)
    iy, ny = lax.axis_index("sp_1"), lax.axis_size("sp_1")
    k = jnp.arange(ny)
    after = lambda last: jnp.sum(
        jnp.where((k[None, :, None] > k[:, None, None]) & (k[None, :, None] < last), logs_y[None], 0.0), 1
    )
    c_in = jnp.where(k[:, None] < iy, jnp.exp(after(iy)), 0.0)
    c_all = jnp.exp(after(ny))
    pieces = got[:, : heads * p].astype(f32).reshape(ny, heads, p, STATE)
    enter_y = jnp.sum(pieces * c_in[:, :, None, None], 0)
    line = jnp.sum(pieces * c_all[:, :, None, None], 0).reshape(heads * p, STATE).astype(bf16)
    line_log = jnp.sum(logs_y, 0)
    before_log = jnp.sum(jnp.where(k[:, None] < iy, logs_y, 0.0), 0)
    hi, mid, lo = split3(line_log)
    logs = jnp.zeros((16, STATE), bf16)
    logs = logs.at[0, :heads].set(hi).at[1, :heads].set(mid).at[2, :heads].set(lo)
    got = spread(jnp.concatenate([line, logs], 0), "sp_0")
    logs_z = jnp.sum(got[:, heads * p : heads * p + 3, :heads].astype(f32), 1)
    iz, nz = lax.axis_index("sp_0"), lax.axis_size("sp_0")
    k = jnp.arange(nz)
    between = jnp.sum(
        jnp.where((k[None, :, None] > k[:, None, None]) & (k[None, :, None] < iz), logs_z[None], 0.0), 1
    )
    c_in = jnp.where(k[:, None] < iz, jnp.exp(between + before_log), 0.0)
    c_init = jnp.exp(jnp.sum(jnp.where(k[:, None] < iz, logs_z, 0.0), 0) + before_log)
    pieces = got[:, : heads * p].astype(f32).reshape(nz, heads, p, STATE)
    start = enter_y + jnp.sum(pieces * c_in[:, :, None, None], 0) + c_init[:, None, None] * initial_state
    start = start.astype(bf16)
    proj = dot(normed, rest[:, : 4 * ch], 1, 0).astype(bf16).astype(f32)
    r_act = jax.nn.silu(causal(proj[:, :ch], fetch_taps, HALO - SHORT + 1, rows)).astype(bf16)
    z_gate = jax.nn.silu(proj[HALO:, ch : 2 * ch])
    glu = proj[:, 2 * ch : 3 * ch] * jax.nn.sigmoid(proj[:, 3 * ch :])
    mix = causal(glu, long_taps, HALO - WIDE + 1, rows)
    sums = jnp.stack([jnp.sum(mix, 1), jnp.sum(mix * mix, 1)])
    sums = jnp.sum(spread(sums, FT), 0)
    mean = sums[0] / C_CH
    var = sums[1] / C_CH - mean * mean
    conv_out = jax.nn.silu((mix - mean[:, None]) * lax.rsqrt(var + EPS)[:, None] * conv_gain).astype(bf16)
    scores = dot(r_act, w16, 1, 1)
    lower = jnp.tril(jnp.ones((rows, rows), bool))
    ys = []
    for h in range(heads):
        gap = jnp.where(lower, cumul[h][:, None] - cumul[h][None, :], 0.0)
        m = jnp.where(lower, jnp.exp(gap) * scores, 0.0).astype(bf16)
        ys.append(dot(m, xs[h], 1, 0) + dot(r_act, start[h], 1, 1) * jnp.exp(cumul[h])[:, None])
    gated = jnp.concatenate(ys, 1) * z_gate
    square = jnp.sum(spread(jnp.sum(gated * gated, 1)[None], FT), (0, 1))
    state_pre = (gated * state_gain).astype(bf16)
    tp = lax.axis_index("tp")

    def half(a):
        a = a.reshape(nf, nt, rows // (nf * nt), *a.shape[1:])
        return lax.dynamic_index_in_dim(a, tp, 1, keepdims=False).reshape(rows // nt, *a.shape[3:])

    def pair(a):
        both = lax.all_gather(a, "tp", axis=0)
        return jnp.concatenate([both[i] for i in range(nt)], 1)

    conv_in = half(pair(conv_out))
    state_in = half(pair(state_pre))
    back_c = pair(rest[:, 4 * ch : 5 * ch])
    back_s = pair(rest[:, 5 * ch :])
    scale = lax.rsqrt(half(square) / D_INNER + EPS)[:, None]
    part = (dot(conv_in, back_c, 1, 1) + scale * dot(state_in, back_s, 1, 1)).astype(bf16)
    pieces = lax.all_to_all(part.reshape(nf, -1, part.shape[1]), "fs", 0, 0, tiled=True)
    return jnp.sum(pieces.astype(f32), 0).astype(bf16)


def solution(mesh):
    torus = Mesh(
        mesh.devices.reshape(8, 8, mesh.shape["fs"], mesh.shape["tp"]), ("sp_0", "sp_1", "fs", "tp")
    )
    w = P(SP, FT)
    in_specs = (
        P(SP, None), P(), w, w, w, w, w, w, P(), P(FT), P(FT), P(FT, SP), P(None, FT), P(None, FT), P(None, FT),
        P(None, FT), P(FT), P(FT), w, w, P(FT, None, None),
    )
    return jax.shard_map(
        per_device, mesh=torus, in_specs=in_specs, out_specs=P((*SP, *FT), None), check_vma=False
    )
```

time: 237 us -> 188 us (0.79)
  blocking collectives: 58.2 us -> 16 us
  waiting for transfers between devices: 97.7 us -> 82.4 us
  matrix products: 15.9 us -> 6.31 us
  local copies, waits for them, and re-layouts: 11.7 us -> 21.2 us
  starting transfers between devices: 33.2 us -> 40 us
  other arithmetic: 4.89 us -> 7.62 us
    all_gather x1 -> x3, waiting for transfers between devices: 83.7 us -> 12.4 us  [the longest x2 12.3 us: pair(): both = lax.all_gather(a, 'tp', axis=0)]
    all_to_all x3 -> x6, waiting for transfers between devices: 13.6 us -> 70 us  [spread(): lax.all_to_all(jnp.broadcast_to(shard[None], (n, *shard.shape)), axis, 0,...]
    all_gather x2, blocking collectives: 40.2 us -> 4.16 us  [pair(): both = lax.all_gather(a, 'tp', axis=0)]
    dot_general x13 -> x12, matrix products: 15.4 us -> 6.31 us  [the longest x11 5.93 us: dot(): lax.dot_general(a, b, (((ca,), (cb,)), ((), ())), preferred_element_type=...]
    slice x7 -> x17, local copies, waits for them, and re-layouts: 0.16 us -> 7.19 us  [the longest x8 3.01 us: pair(): return jnp.concatenate([both[i] for i in range(nt)], 1)]
    all_to_all x1, blocking collectives: 18 us -> 11.9 us  [per_device(): lax.all_to_all(part.reshape(nf, -1, part.shape[1]), 'fs', 0, 0, tiled=True)]
    all_to_all x3 -> x6, starting transfers between devices: 30.4 us -> 35.9 us  [spread(): lax.all_to_all(jnp.broadcast_to(shard[None], (n, *shard.shape)), axis, 0,...]
    broadcast_in_dim x5 -> x6, local copies, waits for them, and re-layouts: 1.84 us -> 4.64 us  [spread(): jnp.broadcast_to(shard[None], (n, *shard.shape))]
  transfers between devices with their start and end apart: 5 -> 10, of which waited for: 5 -> 6; matrix products, arithmetic and copies ran while one was open for 2% -> 14% of each run, Pallas kernels for 0% -> 0%
where the time goes in v1:
time: 188 us; the launch traced here: 187 us
  waiting for transfers between devices  82.4 us (44%)
  starting transfers between devices  40 us (21%)
  local copies, waits for them, and re-layouts  21.2 us (11%)
  blocking collectives  16 us (9%)
  between operations  13.6 us (7%)
  other arithmetic  7.62 us (4%)
  matrix products  6.31 us (3%)
    all_to_all x6, waiting for transfers between devices, spread(): lax.all_to_all(jnp.broadcast_to(shard[None], (n, *shard.shape)), axis, 0,...  70 us
    all_to_all x6, starting transfers between devices, spread(): lax.all_to_all(jnp.broadcast_to(shard[None], (n, *shard.shape)), axis, 0,...  35.9 us
    all_gather x2, waiting for transfers between devices, pair(): both = lax.all_gather(a, 'tp', axis=0)  12.3 us
    all_to_all x1, blocking collectives, per_device(): lax.all_to_all(part.reshape(nf, -1, part.shape[1]), 'fs', 0, 0, tiled=True)  11.9 us
    dot_general x11, matrix products, dot(): lax.dot_general(a, b, (((ca,), (cb,)), ((), ())), preferred_element_type=...  5.93 us
    unnamed x29, local copies, waits for them, and re-layouts  5.31 us
    broadcast_in_dim x6, local copies, waits for them, and re-layouts, spread(): jnp.broadcast_to(shard[None], (n, *shard.shape))  4.64 us
    all_gather x2, blocking collectives, pair(): both = lax.all_gather(a, 'tp', axis=0)  4.16 us
  transfers between devices with their start and end apart: 10, of which 6 were waited for; matrix products, arithmetic and copies ran while one was open for 14% of the time, Pallas kernels for 0%

profile of v1, /device:TPU:1, one launch (start us, length us, event | category | flops | bytes accessed | tf_op | source)
XLA Modules:
  0.0 187.1 jit_solution(15194722190336121326)
XLA Ops:
  6.5 1.0 slice.494
  7.5 4.0 %collective-permute-start = (bf16[32,2048]{1,0:T(8,128)(2,1)S(1)}, bf16[32,2048]{1,0:T(8,128)(2,1)S(1)}, u32[]{:S(2)}, u32[]{:S(2)}) collective-permute-start(bf16[32,2048]{1,0:T(8,128)(2,1)S(1)} %slice.494), channel_id=1, source_target_pairs={{0,8},{8,16},{16,24},{24,32},{32,40},{40,48},{48,56},{56,64},{64,7... | collective-permute-start | bytes 393224 | tf_op jit(solution)/shard_map/ppermute | solution.py:27
  11.6 0.7 constant_dynamic-update-slice_fusion.7
  12.3 0.7 constant_dynamic-update-slice_fusion.6
  13.0 0.7 constant_dynamic-update-slice_fusion.5
  13.7 0.7 constant_dynamic-update-slice_fusion.4
  14.4 0.7 constant_dynamic-update-slice_fusion.3
  15.1 0.7 constant_dynamic-update-slice_fusion.2
  15.8 0.7 constant_dynamic-update-slice_fusion.1
  16.5 0.7 constant_dynamic-update-slice_fusion
  17.2 0.8 broadcast_in_dim.143
  18.1 5.9 %all-to-all-start = ((bf16[8,32,1024]{2,1,0:T(8,128)(2,1)}), bf16[8,32,1024]{2,1,0:T(8,128)(2,1)S(1)}, u32[]{:S(2)}, u32[]{:S(2)}) async-start(bf16[8,32,1024]{2,1,0:T(8,128)(2,1)} %broadcast_in_dim.143), calls=%async_computation | async-start | bytes 1048576 | tf_op jit(solution)/shard_map/all_to_all | solution.py:22
  24.0 0.8 slice_bitcast_fusion.17
  24.8 0.8 slice_bitcast_fusion.9
  25.7 0.7 exponential_negate_fusion
  27.1 13.3 %all-to-all-done = bf16[8,32,1024]{2,1,0:T(8,128)(2,1)S(1)} async-done(((bf16[8,32,1024]{2,1,0:T(8,128)(2,1)}), bf16[8,32,1024]{2,1,0:T(8,128)(2,1)S(1)}, u32[]{:S(2)}, u32[]{:S(2)}) %all-to-all-start) | async-done | bytes 524320 | tf_op jit(solution)/shard_map/all_to_all | solution.py:22
  40.4 1.1 broadcast_in_dim.146
  41.4 10.7 %all-to-all-start.2 = ((bf16[8,256,256]{2,1,0:T(8,128)(2,1)}), bf16[8,256,256]{2,1,0:T(8,128)(2,1)S(1)}, u32[]{:S(2)}, u32[]{:S(2)}) async-start(bf16[8,256,256]{2,1,0:T(8,128)(2,1)} %broadcast_in_dim.146), calls=%async_computation.2 | async-start | bytes 2097152 | tf_op jit(solution)/shard_map/all_to_all | solution.py:22
  52.2 0.4 fusion.16
  52.7 0.6 reduce-window.6
  53.9 0.8 slice.625
  55.2 30.6 %all-to-all-done.2 = bf16[8,256,256]{2,1,0:T(8,128)(2,1)S(1)} async-done(((bf16[8,256,256]{2,1,0:T(8,128)(2,1)}), bf16[8,256,256]{2,1,0:T(8,128)(2,1)S(1)}, u32[]{:S(2)}, u32[]{:S(2)}) %all-to-all-start.2) | async-done | bytes 1048608 | tf_op jit(solution)/shard_map/all_to_all | solution.py:22
  85.8 0.8 fusion.13
  86.6 0.5 divide_multiply_fusion
  87.4 0.8 broadcast_in_dim.147
  88.2 3.4 %all-to-all-start.3 = ((bf16[8,144,128]{2,1,0:T(8,128)(2,1)}), bf16[8,144,128]{2,1,0:T(8,128)(2,1)S(1)}, u32[]{:S(2)}, u32[]{:S(2)}) async-start(bf16[8,144,128]{2,1,0:T(8,128)(2,1)} %broadcast_in_dim.147), calls=%async_computation.3 | async-start | bytes 589824 | tf_op jit(solution)/shard_map/all_to_all | solution.py:22
  91.7 11.5 %all-to-all-done.3 = bf16[8,144,128]{2,1,0:T(8,128)(2,1)S(1)} async-done(((bf16[8,144,128]{2,1,0:T(8,128)(2,1)}), bf16[8,144,128]{2,1,0:T(8,128)(2,1)S(1)}, u32[]{:S(2)}, u32[]{:S(2)}) %all-to-all-start.3) | async-done | bytes 294944 | tf_op jit(solution)/shard_map/all_to_all | solution.py:22
  104.5 0.3 fusion.26
  104.8 0.8 broadcast_in_dim.154
  105.6 3.4 %all-to-all-start.4 = ((bf16[8,144,128]{2,1,0:T(8,128)(2,1)}), bf16[8,144,128]{2,1,0:T(8,128)(2,1)S(1)}, u32[]{:S(2)}, u32[]{:S(2)}) async-start(bf16[8,144,128]{2,1,0:T(8,128)(2,1)} %broadcast_in_dim.154), calls=%async_computation.4 | async-start | bytes 589824 | tf_op jit(solution)/shard_map/all_to_all | solution.py:22
  109.1 10.1 %all-to-all-done.4 = bf16[8,144,128]{2,1,0:T(8,128)(2,1)S(1)} async-done(((bf16[8,144,128]{2,1,0:T(8,128)(2,1)}), bf16[8,144,128]{2,1,0:T(8,128)(2,1)S(1)}, u32[]{:S(2)}, u32[]{:S(2)}) %all-to-all-start.4) | async-done | bytes 294944 | tf_op jit(solution)/shard_map/all_to_all | solution.py:22
  120.2 2.9 %fusion.10 = f32[288,512]{0,1:T(8,128)S(1)} fusion(bf16[288,2048]{1,0:T(8,128)(2,1)S(1)} %fusion.4, bf16[2048,768]{1,0:T(8,128)(2,1)} %all-gather.8.cloned.1.call-done), kind=kOutput, calls=%fused_computation.11 | convolution fusion | flops 604274688 | bytes 3866624 | tf_op jit(solution)/shard_map/dot_general | solution.py:31
  124.6 0.6 broadcast_in_dim.158
  125.2 7.6 %all-to-all-start.5 = ((f32[8,1,256]{2,1,0:T(1,128)}), f32[8,1,256]{2,1,0:T(1,128)S(1)}, u32[]{:S(2)}, u32[]{:S(2)}) async-start(f32[8,1,256]{2,1,0:T(1,128)} %broadcast_in_dim.158), calls=%async_computation.5 | async-start | bytes 16384 | tf_op jit(solution)/shard_map/all_to_all | solution.py:22
  132.8 2.3 %fusion.98 = (bf16[2048,128]{1,0:T(8,128)(2,1)}, bf16[2048,128]{1,0:T(8,128)(2,1)}) fusion(bf16[2048,768]{1,0:T(8,128)(2,1)} %all-gather.8.cloned.1.call-done), kind=kLoop, calls=%fused_computation.256 | loop fusion | bytes 2097152 | tf_op jit(solution)/shard_map/slice | solution.py:150
  135.2 1.9 %all-gather.2 = bf16[512,128]{0,1:T(8,128)(2,1)S(1)} all-gather(bf16[256,128]{0,1:T(8,128)(2,1)S(1)} %multiply_convert_fusion), channel_id=4, replica_groups=mesh['sp_0'=8,'sp_1'=8,'fs'=4,'tp'=2] {'tp'}, dimensions={0}, use_global_device_ids=true | all-gather | bytes 196608 | tf_op jit(solution)/shard_map/all_gather | solution.py:144
  137.2 1.8 fusion.96
  139.3 0.6 broadcast_in_dim.144
  140.0 4.8 %all-to-all-start.1 = ((f32[8,2,256]{2,1,0:T(2,128)}), f32[8,2,256]{2,1,0:T(2,128)S(1)}, u32[]{:S(2)}, u32[]{:S(2)}) async-start(f32[8,2,256]{2,1,0:T(2,128)} %broadcast_in_dim.144), calls=%async_computation.1 | async-start | bytes 32768 | tf_op jit(solution)/shard_map/all_to_all | solution.py:22
  145.0 4.4 %all-to-all-done.1 = f32[8,2,256]{2,1,0:T(2,128)S(1)} async-done(((f32[8,2,256]{2,1,0:T(2,128)}), f32[8,2,256]{2,1,0:T(2,128)S(1)}, u32[]{:S(2)}, u32[]{:S(2)}) %all-to-all-start.1) | async-done | bytes 16416 | tf_op jit(solution)/shard_map/all_to_all | solution.py:22
  149.6 2.3 %all-gather = bf16[512,128]{0,1:T(8,128)(2,1)S(1)} all-gather(bf16[256,128]{0,1:T(8,128)(2,1)S(1)} %multiply_convert_fusion.4), channel_id=2, replica_groups=mesh['sp_0'=8,'sp_1'=8,'fs'=4,'tp'=2] {'tp'}, dimensions={0}, use_global_device_ids=true | all-gather | bytes 196608 | tf_op jit(solution)/shard_map/all_gather | solution.py:144
  152.2 1.3 fusion.100
  153.4 0.5 fusion.18
  153.9 12.3 %all-gather.12.cloned.1.call-done = bf16[4096,128]{1,0:T(8,128)(2,1)} async-done(((bf16[2048,128]{1,0:T(8,128)(2,1)}), bf16[4096,128]{1,0:T(8,128)(2,1)}) %all-gather.12.cloned.1.call-update) | async-done | bytes 1048592 | tf_op jit(solution)/shard_map/all_gather | solution.py:144
  166.2 1.3 fusion.99
  167.5 0.5 fusion.1
  168.0 11.9 %all_to_all.35 = bf16[4,32,2048]{2,1,0:T(8,128)(2,1)S(1)} all-to-all(bf16[4,32,2048]{2,1,0:T(8,128)(2,1)S(1)} %bitcast.172), channel_id=1, replica_groups=mesh['sp_0'=8,'sp_1'=8,'fs'=4,'tp'=2] {'fs'}, dimensions={0} | all-to-all | bytes 1048576 | tf_op jit(solution)/shard_map/all_to_all | solution.py:153
  179.8 0.7 reduce_sum.185
  (117 shorter events, 7.1 us)
Async XLA Ops:
  6.5 45.7 %copy-start = (bf16[2048,16]{0,1:T(8,128)(2,1)S(1)}, bf16[2048,16]{0,1:T(8,128)(2,1)}, u32[]{:S(2)}) copy-start(bf16[2048,16]{0,1:T(8,128)(2,1)} %param.41) | copy-start | bytes 196612
  6.5 19.8 %copy-start.1 = (bf16[256,2048]{1,0:T(8,128)(2,1)S(1)}, bf16[256,2048]{1,0:T(8,128)(2,1)}, u32[]{:S(2)}) copy-start(bf16[256,2048]{1,0:T(8,128)(2,1)} %param.33) | copy-start | bytes 3145732
  6.5 20.2 %copy-start.4 = (f32[2048]{0:T(1024)S(1)}, f32[2048]{0:T(1024)}, u32[]{:S(2)}) copy-start(f32[2048]{0:T(1024)} %param.34) | copy-start | bytes 24580
  7.5 18.8 %collective-permute-start = (bf16[32,2048]{1,0:T(8,128)(2,1)S(1)}, bf16[32,2048]{1,0:T(8,128)(2,1)S(1)}, u32[]{:S(2)}, u32[]{:S(2)}) collective-permute-start(bf16[32,2048]{1,0:T(8,128)(2,1)S(1)} %slice.494), channel_id=1, source_target_pairs={{0,8},{8,16},{16,24},{24,32},{32,40},{40,48},{48,56},{56,64},{64,7... | collective-permute-start | bytes 393224 | tf_op jit(solution)/shard_map/ppermute | solution.py:27
  18.1 22.3 %all-to-all-start = ((bf16[8,32,1024]{2,1,0:T(8,128)(2,1)}), bf16[8,32,1024]{2,1,0:T(8,128)(2,1)S(1)}, u32[]{:S(2)}, u32[]{:S(2)}) async-start(bf16[8,32,1024]{2,1,0:T(8,128)(2,1)} %broadcast_in_dim.143), calls=%async_computation | async-start | bytes 1048576 | tf_op jit(solution)/shard_map/all_to_all | solution.py:22
  40.4 12.2 %copy-start.5 = (f32[2,256]{1,0:T(2,128)S(1)}, f32[2,256]{1,0:T(2,128)}, u32[]{:S(2)}) copy-start(f32[2,256]{1,0:T(2,128)} %param.44) | copy-start | bytes 6148
  40.4 12.2 %copy-start.8 = (f32[2]{0:T(128)S(1)}, f32[2]{0:T(128)}, u32[]{:S(2)}) copy-start(f32[2]{0:T(128)} %param.42) | copy-start | bytes 28
  41.4 44.4 %all-to-all-start.2 = ((bf16[8,256,256]{2,1,0:T(8,128)(2,1)}), bf16[8,256,256]{2,1,0:T(8,128)(2,1)S(1)}, u32[]{:S(2)}, u32[]{:S(2)}) async-start(bf16[8,256,256]{2,1,0:T(8,128)(2,1)} %broadcast_in_dim.146), calls=%async_computation.2 | async-start | bytes 2097152 | tf_op jit(solution)/shard_map/all_to_all | solution.py:22
  52.2 68.0 %all-gather.8.cloned.1.call-start = ((), (), s32[]{:S(2)}) async-start(), calls=%async_computation.7 | async-start | bytes 3538944 | tf_op jit(solution)/shard_map/all_gather | solution.py:65
  85.8 5.8 %copy-start.3 = (f32[31,128]{1,0:T(8,128)S(1)}, f32[31,128]{1,0:T(8,128)}, u32[]{:S(2)}) copy-start(f32[31,128]{1,0:T(8,128)} %param.48) | copy-start | bytes 47620
  87.1 33.0 %copy-start.2 = (f32[2,64,128]{2,1,0:T(8,128)S(1)}, f32[2,64,128]{2,1,0:T(8,128)}, u32[]{:S(2)}) copy-start(f32[2,64,128]{2,1,0:T(8,128)} %param.53) | copy-start | bytes 196612
  88.2 15.0 %all-to-all-start.3 = ((bf16[8,144,128]{2,1,0:T(8,128)(2,1)}), bf16[8,144,128]{2,1,0:T(8,128)(2,1)S(1)}, u32[]{:S(2)}, u32[]{:S(2)}) async-start(bf16[8,144,128]{2,1,0:T(8,128)(2,1)} %broadcast_in_dim.147), calls=%async_computation.3 | async-start | bytes 589824 | tf_op jit(solution)/shard_map/all_to_all | solution.py:22
  105.6 13.7 %all-to-all-start.4 = ((bf16[8,144,128]{2,1,0:T(8,128)(2,1)}), bf16[8,144,128]{2,1,0:T(8,128)(2,1)S(1)}, u32[]{:S(2)}, u32[]{:S(2)}) async-start(bf16[8,144,128]{2,1,0:T(8,128)(2,1)} %broadcast_in_dim.154), calls=%async_computation.4 | async-start | bytes 589824 | tf_op jit(solution)/shard_map/all_to_all | solution.py:22
  123.9 11.2 %copy-start.6 = (f32[128]{0:T(128)S(1)}, f32[128]{0:T(128)}, u32[]{:S(2)}) copy-start(f32[128]{0:T(128)} %param.50) | copy-start | bytes 1540
  125.2 14.2 %all-to-all-start.5 = ((f32[8,1,256]{2,1,0:T(1,128)}), f32[8,1,256]{2,1,0:T(1,128)S(1)}, u32[]{:S(2)}, u32[]{:S(2)}) async-start(f32[8,1,256]{2,1,0:T(1,128)} %broadcast_in_dim.158), calls=%async_computation.5 | async-start | bytes 16384 | tf_op jit(solution)/shard_map/all_to_all | solution.py:22
  132.8 19.4 %all-gather.10.cloned.1.call-start = ((), (), s32[]{:S(2)}) async-start(), calls=%async_computation.8 | async-start | bytes 1572864 | tf_op jit(solution)/shard_map/all_gather | solution.py:144
  135.1 31.2 %all-gather.12.cloned.1.call-start = ((), (), s32[]{:S(2)}) async-start(), calls=%async_computation.9 | async-start | bytes 1572864 | tf_op jit(solution)/shard_map/all_gather | solution.py:144
  137.2 12.3 %copy-start.7 = (f32[128]{0:T(128)S(1)}, f32[128]{0:T(128)}, u32[]{:S(2)}) copy-start(f32[128]{0:T(128)} %param.49) | copy-start | bytes 1540
  140.0 9.5 %all-to-all-start.1 = ((f32[8,2,256]{2,1,0:T(2,128)}), f32[8,2,256]{2,1,0:T(2,128)S(1)}, u32[]{:S(2)}, u32[]{:S(2)}) async-start(f32[8,2,256]{2,1,0:T(2,128)} %broadcast_in_dim.144), calls=%async_computation.1 | async-start | bytes 32768 | tf_op jit(solution)/shard_map/all_to_all | solution.py:22
Sparse Core Ops, SparseCore 0:
  55.0 53.0 all-gather.7
  135.7 9.9 all-gather.9
  147.7 18.4 all-gather.11

commit v2 on v1

--- a/solution.py
+++ b/solution.py
@@ -1,6 +1,8 @@
 import jax
 import jax.numpy as jnp
 from jax import lax
+from jax.experimental import pallas as pl
+from jax.experimental.pallas import tpu as pltpu
 from jax.sharding import Mesh
 from jax.sharding import PartitionSpec as P
 
@@ -48,6 +50,39 @@
     return hi, mid, (rest - mid.astype(f32)).astype(bf16)
 
 
+def lay_out(early, late, n_all, n_y):
+    rows, ch = early[0].shape
+    ne, nl = len(early), len(late)
+
+    def body(*refs):
+        ins, (first, rest) = refs[: ne + nl], refs[ne + nl :]
+        for i in range(nl):
+            w = ins[ne + i][...]
+            for k in range(n_y):
+                rest[k, :, i * ch : (i + 1) * ch] = w
+        for i in range(ne):
+            w = ins[i][...]
+            for k in range(n_all):
+                first[k, :, i * ch : (i + 1) * ch] = w
+
+    return pl.pallas_call(
+        body,
+        out_shape=(
+            jax.ShapeDtypeStruct((n_all, rows, ne * ch), bf16),
+            jax.ShapeDtypeStruct((n_y, rows, nl * ch), bf16),
+        ),
+        in_specs=[pl.BlockSpec(memory_space=pltpu.VMEM)] * (ne + nl),
+        out_specs=(pl.BlockSpec(memory_space=pltpu.VMEM),) * 2,
+        name="lay_out",
+    )(*early, *late)
+
+
+def log_rows(logs):
+    hi, mid, lo = split3(logs)
+    rows = jnp.stack([hi, mid, lo])
+    return jnp.pad(rows, ((0, 13), (0, STATE - logs.shape[0])))
+
+
 def per_device(
     tokens, norm_gain, conv_value, conv_gate, mixer_gate, state_input, write_projection, state_read,
     step_proj, step_bias, decay_log, decay_extra, input_taps, write_taps, fetch_taps, long_taps,
@@ -58,17 +93,21 @@
     heads = step_bias.shape[0]
     p = ch // heads
     nf, nt = lax.axis_size("fs"), lax.axis_size("tp")
-    shard = jnp.concatenate(
-        [state_input, write_projection, state_read, mixer_gate, conv_value, conv_gate, conv_output, state_output], 1
-    )
-    near = spread(shard, "sp_1").reshape(-1, 8 * ch)
-    rest = lax.all_gather(near[:, 2 * ch :], "sp_0", axis=0, tiled=True)
-    first = spread(near[:, : 2 * ch], "sp_0").reshape(-1, 2 * ch)
+    first, rest = lay_out(
+        (state_input, write_projection),
+        (state_read, mixer_gate, conv_value, conv_gate, conv_output, state_output),
+        lax.axis_size(SP),
+        lax.axis_size("sp_1"),
+    )
+    rest = lax.all_to_all(rest, "sp_1", 0, 0, tiled=True).reshape(-1, 6 * ch)
+    rest = lax.all_gather(rest, "sp_0", axis=0, tiled=True)
+    first = lax.all_to_all(first, SP, 0, 0, tiled=True).reshape(-1, 2 * ch)
     halo = previous(tokens[rows - HALO :])
     normed = unit_rows(jnp.concatenate([halo, tokens], 0), norm_gain)
     own = normed[HALO:]
     step_all = jnp.dot(own, step_proj, preferred_element_type=f32)
-    me = lax.axis_index("fs") * nt + lax.axis_index("tp")
+    tp = lax.axis_index("tp")
+    me = lax.axis_index("fs") * nt + tp
     step = jax.nn.softplus(lax.dynamic_slice_in_dim(step_all, me * heads, heads, 1) + step_bias)
     log_step = (-jnp.exp(decay_log) * step + decay_extra.T).T
     cumul = jnp.cumsum(log_step, axis=1)
@@ -82,10 +121,7 @@
     ends = jnp.concatenate(
         [dot(xs[h], (w_act * left[:, h : h + 1]).astype(bf16), 0, 0) for h in range(heads)], 0
     ).astype(bf16)
-    hi, mid, lo = split3(total)
-    logs = jnp.zeros((16, STATE), bf16)
-    logs = logs.at[0, :heads].set(hi).at[1, :heads].set(mid).at[2, :heads].set(lo)
-    got = spread(jnp.concatenate([ends, logs], 0), "sp_1")
+    got = spread(jnp.concatenate([ends, log_rows(total)], 0), "sp_1")
     logs_y = jnp.sum(got[:, heads * p : heads * p + 3, :heads].astype(f32), 1)
     iy, ny = lax.axis_index("sp_1"), lax.axis_size("sp_1")
     k = jnp.arange(ny)
@@ -99,10 +135,7 @@
     line = jnp.sum(pieces * c_all[:, :, None, None], 0).reshape(heads * p, STATE).astype(bf16)
     line_log = jnp.sum(logs_y, 0)
     before_log = jnp.sum(jnp.where(k[:, None] < iy, logs_y, 0.0), 0)
-    hi, mid, lo = split3(line_log)
-    logs = jnp.zeros((16, STATE), bf16)
-    logs = logs.at[0, :heads].set(hi).at[1, :heads].set(mid).at[2, :heads].set(lo)
-    got = spread(jnp.concatenate([line, logs], 0), "sp_0")
+    got = spread(jnp.concatenate([line, log_rows(line_log)], 0), "sp_0")
     logs_z = jnp.sum(got[:, heads * p : heads * p + 3, :heads].astype(f32), 1)
     iz, nz = lax.axis_index("sp_0"), lax.axis_size("sp_0")
     k = jnp.arange(nz)
@@ -114,43 +147,43 @@
     pieces = got[:, : heads * p].astype(f32).reshape(nz, heads, p, STATE)
     start = enter_y + jnp.sum(pieces * c_in[:, :, None, None], 0) + c_init[:, None, None] * initial_state
     start = start.astype(bf16)
+    back = rest[:, 4 * ch :]
+    back_other = lax.ppermute(back, "tp", [(i, nt - 1 - i) for i in range(nt)])
+    gain_both = lax.all_gather(conv_gain, "tp")
     proj = dot(normed, rest[:, : 4 * ch], 1, 0).astype(bf16).astype(f32)
     r_act = jax.nn.silu(causal(proj[:, :ch], fetch_taps, HALO - SHORT + 1, rows)).astype(bf16)
     z_gate = jax.nn.silu(proj[HALO:, ch : 2 * ch])
     glu = proj[:, 2 * ch : 3 * ch] * jax.nn.sigmoid(proj[:, 3 * ch :])
     mix = causal(glu, long_taps, HALO - WIDE + 1, rows)
-    sums = jnp.stack([jnp.sum(mix, 1), jnp.sum(mix * mix, 1)])
-    sums = jnp.sum(spread(sums, FT), 0)
-    mean = sums[0] / C_CH
-    var = sums[1] / C_CH - mean * mean
-    conv_out = jax.nn.silu((mix - mean[:, None]) * lax.rsqrt(var + EPS)[:, None] * conv_gain).astype(bf16)
     scores = dot(r_act, w16, 1, 1)
     lower = jnp.tril(jnp.ones((rows, rows), bool))
-    ys = []
+    inner = []
     for h in range(heads):
         gap = jnp.where(lower, cumul[h][:, None] - cumul[h][None, :], 0.0)
         m = jnp.where(lower, jnp.exp(gap) * scores, 0.0).astype(bf16)
-        ys.append(dot(m, xs[h], 1, 0) + dot(r_act, start[h], 1, 1) * jnp.exp(cumul[h])[:, None])
+        inner.append(dot(m, xs[h], 1, 0))
+    ys = [inner[h] + dot(r_act, start[h], 1, 1) * jnp.exp(cumul[h])[:, None] for h in range(heads)]
     gated = jnp.concatenate(ys, 1) * z_gate
-    square = jnp.sum(spread(jnp.sum(gated * gated, 1)[None], FT), (0, 1))
-    state_pre = (gated * state_gain).astype(bf16)
-    tp = lax.axis_index("tp")
+    sums = jnp.stack([jnp.sum(mix, 1), jnp.sum(mix * mix, 1), jnp.sum(gated * gated, 1)])
+    sums = jnp.sum(spread(sums, FT), 0)
 
     def half(a):
         a = a.reshape(nf, nt, rows // (nf * nt), *a.shape[1:])
         return lax.dynamic_index_in_dim(a, tp, 1, keepdims=False).reshape(rows // nt, *a.shape[3:])
 
-    def pair(a):
-        both = lax.all_gather(a, "tp", axis=0)
-        return jnp.concatenate([both[i] for i in range(nt)], 1)
-
-    conv_in = half(pair(conv_out))
-    state_in = half(pair(state_pre))
-    back_c = pair(rest[:, 4 * ch : 5 * ch])
-    back_s = pair(rest[:, 5 * ch :])
-    scale = lax.rsqrt(half(square) / D_INNER + EPS)[:, None]
-    part = (dot(conv_in, back_c, 1, 1) + scale * dot(state_in, back_s, 1, 1)).astype(bf16)
-    pieces = lax.all_to_all(part.reshape(nf, -1, part.shape[1]), "fs", 0, 0, tiled=True)
+    pre = jnp.concatenate([mix.astype(bf16), (gated * state_gain).astype(bf16)], 1)
+    both = lax.all_gather(pre, "tp", axis=0)
+    sums = half(sums.T)
+    mean = sums[:, 0:1] / C_CH
+    rstd = lax.rsqrt(sums[:, 1:2] / C_CH - mean * mean + EPS)
+    scale = lax.rsqrt(sums[:, 2:3] / D_INNER + EPS)
+    part = 0.0
+    for i, w in ((tp, back), (1 - tp, back_other)):
+        a = half(lax.dynamic_index_in_dim(both, i, 0, keepdims=False)).astype(f32)
+        g = lax.dynamic_index_in_dim(gain_both, i, 0, keepdims=False)
+        conv = jax.nn.silu((a[:, :ch] - mean) * rstd * g)
+        part = part + dot(jnp.concatenate([conv, a[:, ch:] * scale], 1).astype(bf16), w, 1, 1)
+    pieces = lax.all_to_all(part.astype(bf16).reshape(nf, -1, part.shape[1]), "fs", 0, 0, tiled=True)
     return jnp.sum(pieces.astype(f32), 0).astype(bf16)
 
 

time: 188 us -> 156 us (0.83)
  waiting for transfers between devices: 82.4 us -> 54.3 us
  local copies, waits for them, and re-layouts: 21.2 us -> 8.67 us
  matrix products: 6.31 us -> 8.77 us
  Pallas kernels: 0 us -> 2.11 us
  blocking collectives: 16 us -> 18 us
    all_to_all x6 -> x3, waiting for transfers between devices: 70 us -> 23.2 us  [spread(): lax.all_to_all(jnp.broadcast_to(shard[None], (n, *shard.shape)), axis, 0,...]
    all_to_all x0 -> x2, waiting for transfers between devices: none -> 29.1 us  [the longest x1 23.6 us: per_device(): first = lax.all_to_all(first, SP, 0, 0, tiled=True).reshape(-1, 2 * ch)]
    all_to_all x6 -> x3, starting transfers between devices: 35.9 us -> 16.1 us  [spread(): lax.all_to_all(jnp.broadcast_to(shard[None], (n, *shard.shape)), axis, 0,...]
    all_to_all x0 -> x2, starting transfers between devices: none -> 18.6 us  [the longest x1 12.7 us: per_device(): first = lax.all_to_all(first, SP, 0, 0, tiled=True).reshape(-1, 2 * ch)]
    all_gather x3 -> x1, waiting for transfers between devices: 12.4 us -> 0.02 us  [per_device(): rest = lax.all_gather(rest, 'sp_0', axis=0, tiled=True)]
    unnamed x29 -> x24, local copies, waits for them, and re-layouts: 5.31 us -> 0.4 us
    slice x11 -> x2, local copies, waits for them, and re-layouts: 6.09 us -> 1.22 us  [the longest x1 1.06 us: per_device(): back = rest[:, 4 * ch:]]
    broadcast_in_dim x6 -> x3, local copies, waits for them, and re-layouts: 4.64 us -> 2.15 us  [spread(): jnp.broadcast_to(shard[None], (n, *shard.shape))]
  transfers between devices with their start and end apart: 10 -> 8, of which waited for: 6 -> 5; matrix products, arithmetic and copies ran while one was open for 14% -> 10% of each run, Pallas kernels for 0% -> 1%
where the time goes in v2:
time: 156 us; the launch traced here: 155 us
  waiting for transfers between devices  54.3 us (35%)
  starting transfers between devices  40.8 us (26%)
  blocking collectives  18 us (12%)
  between operations  13.9 us (9%)
  other arithmetic  8.83 us (6%)
  matrix products  8.77 us (6%)
  local copies, waits for them, and re-layouts  8.67 us (6%)
  Pallas kernels  2.11 us (1%)
    all_to_all x1, waiting for transfers between devices, per_device(): first = lax.all_to_all(first, SP, 0, 0, tiled=True).reshape(-1, 2 * ch)  23.6 us
    all_to_all x3, waiting for transfers between devices, spread(): lax.all_to_all(jnp.broadcast_to(shard[None], (n, *shard.shape)), axis, 0,...  23.2 us
    all_to_all x3, starting transfers between devices, spread(): lax.all_to_all(jnp.broadcast_to(shard[None], (n, *shard.shape)), axis, 0,...  16.1 us
    all_to_all x1, starting transfers between devices, per_device(): first = lax.all_to_all(first, SP, 0, 0, tiled=True).reshape(-1, 2 * ch)  12.7 us
    all_to_all x1, blocking collectives, per_device(): lax.all_to_all(part.astype(bf16).reshape(nf, -1, part.shape[1]), 'fs', 0,...  12.6 us
    dot_general x11, matrix products, dot(): lax.dot_general(a, b, (((ca,), (cb,)), ((), ())), preferred_element_type=...  8.39 us
    all_to_all x1, starting transfers between devices, per_device(): rest = lax.all_to_all(rest, 'sp_1', 0, 0, tiled=True).reshape(-1, 6 * ch)  5.92 us
    all_to_all x1, waiting for transfers between devices, per_device(): rest = lax.all_to_all(rest, 'sp_1', 0, 0, tiled=True).reshape(-1, 6 * ch)  5.56 us
  transfers between devices with their start and end apart: 8, of which 5 were waited for; matrix products, arithmetic and copies ran while one was open for 10% of the time, Pallas kernels for 1%

profile of v2, /device:TPU:1, one launch (start us, length us, event | category | flops | bytes accessed | tf_op | source)
XLA Modules:
  0.0 155.3 jit_solution(13616412447617286086)
XLA Ops:
  6.5 1.0 slice.372
  7.5 4.0 %collective-permute-start = (bf16[32,2048]{1,0:T(8,128)(2,1)S(1)}, bf16[32,2048]{1,0:T(8,128)(2,1)S(1)}, u32[]{:S(2)}, u32[]{:S(2)}) collective-permute-start(bf16[32,2048]{1,0:T(8,128)(2,1)S(1)} %slice.372), channel_id=1, source_target_pairs={{0,8},{8,16},{16,24},{24,32},{32,40},{40,48},{48,56},{56,64},{64,7... | collective-permute-start | bytes 393224 | tf_op jit(solution)/shard_map/ppermute | solution.py:29
  11.6 2.1 %lay_out.1 = (bf16[64,32,256]{2,1,0:T(8,128)(2,1)}, bf16[8,32,768]{2,1,0:T(8,128)(2,1)}) custom-call(bf16[32,128]{1,0:T(8,128)(2,1)} %refs_0_.1, bf16[32,128]{1,0:T(8,128)(2,1)} %refs_1_.1, bf16[32,128]{1,0:T(8,128)(2,1)} %refs_2_.1, bf16[32,128]{1,0:T(8,128)(2,1)} %refs_3_.1, bf16[32,128]{1,0:T(8,128)(2,1)} %refs_4_.1, bf16[32,128]{1,0:T(8,128)(2,1)} %refs_5_.1, ...), custom_call_target="tpu_custom_call" | custom-call | tf_op jit(solution)/shard_map/lay_out/pallas_call | solution.py:68
  13.7 5.9 %all-to-all-start = ((bf16[8,32,768]{2,1,0:T(8,128)(2,1)}), bf16[8,32,768]{2,1,0:T(8,128)(2,1)S(1)}, u32[]{:S(2)}, u32[]{:S(2)}) async-start(bf16[8,32,768]{2,1,0:T(8,128)(2,1)} %get-tuple-element.7), calls=%async_computation | async-start | bytes 786432 | tf_op jit(solution)/shard_map/all_to_all | solution.py:102
  19.6 0.8 slice_bitcast_fusion.17
  20.5 3.3 %all-gather.2 = f32[2,1,128]{2,1,0:T(1,128)S(1)} all-gather(f32[1,1,128]{2,1,0:T(1,128)} %bitcast.207), channel_id=3, replica_groups=mesh['sp_0'=8,'sp_1'=8,'fs'=4,'tp'=2] {'tp'}, dimensions={0}, use_global_device_ids=true | all-gather | bytes 1536 | tf_op jit(solution)/shard_map/all_gather | solution.py:152
  23.7 0.8 slice_bitcast_fusion.9
  24.6 0.7 exponential_negate_fusion
  25.3 1.5 fusion.1
  26.8 5.6 %all-to-all-done = bf16[8,32,768]{2,1,0:T(8,128)(2,1)S(1)} async-done(((bf16[8,32,768]{2,1,0:T(8,128)(2,1)}), bf16[8,32,768]{2,1,0:T(8,128)(2,1)S(1)}, u32[]{:S(2)}, u32[]{:S(2)}) %all-to-all-start) | async-done | bytes 393248 | tf_op jit(solution)/shard_map/all_to_all | solution.py:102
  32.4 12.7 %all-to-all-start.1 = ((bf16[64,32,256]{2,1,0:T(8,128)(2,1)}), bf16[64,32,256]{2,1,0:T(8,128)(2,1)}, u32[]{:S(2)}, u32[]{:S(2)}) async-start(bf16[64,32,256]{2,1,0:T(8,128)(2,1)} %get-tuple-element.8), calls=%async_computation.1 | async-start | bytes 2097152 | tf_op jit(solution)/shard_map/all_to_all | solution.py:104
  45.2 0.3 fusion.3
  45.5 0.4 fusion.15
  46.0 0.6 reduce-window.6
  46.7 0.2 slice_reduce_fusion
  46.8 0.2 reduce-window.9
  47.4 23.6 %all-to-all-done.1 = bf16[64,32,256]{2,1,0:T(8,128)(2,1)} async-done(((bf16[64,32,256]{2,1,0:T(8,128)(2,1)}), bf16[64,32,256]{2,1,0:T(8,128)(2,1)}, u32[]{:S(2)}, u32[]{:S(2)}) %all-to-all-start.1) | async-done | bytes 1048608 | tf_op jit(solution)/shard_map/all_to_all | solution.py:104
  71.0 2.0 %fusion.12 = f32[288,256]{0,1:T(8,128)S(1)} fusion(bf16[288,2048]{1,0:T(8,128)(2,1)S(1)} %fusion.3, bf16[2048,256]{1,0:T(8,128)(2,1)} %bitcast.39), kind=kOutput, calls=%fused_computation.13 | convolution fusion | flops 302137344 | bytes 2523136 | tf_op jit(solution)/shard_map/dot_general | solution.py:33
  73.0 0.5 divide_multiply_fusion
  73.5 0.1 convolution_convert_fusion.2
  73.7 0.2 convolution_convert_fusion.1
  73.8 0.8 broadcast_in_dim.125
  74.6 5.7 %all-to-all-start.2 = ((bf16[8,144,128]{2,1,0:T(8,128)(2,1)}), bf16[8,144,128]{2,1,0:T(8,128)(2,1)S(1)}, u32[]{:S(2)}, u32[]{:S(2)}) async-start(bf16[8,144,128]{2,1,0:T(8,128)(2,1)} %broadcast_in_dim.125), calls=%async_computation.2 | async-start | bytes 589824 | tf_op jit(solution)/shard_map/all_to_all | solution.py:24
  80.4 9.7 %all-to-all-done.2 = bf16[8,144,128]{2,1,0:T(8,128)(2,1)S(1)} async-done(((bf16[8,144,128]{2,1,0:T(8,128)(2,1)}), bf16[8,144,128]{2,1,0:T(8,128)(2,1)S(1)}, u32[]{:S(2)}, u32[]{:S(2)}) %all-to-all-start.2) | async-done | bytes 294944 | tf_op jit(solution)/shard_map/all_to_all | solution.py:24
  91.1 0.3 fusion.18
  91.4 0.8 broadcast_in_dim.132
  92.2 3.6 %all-to-all-start.3 = ((bf16[8,144,128]{2,1,0:T(8,128)(2,1)}), bf16[8,144,128]{2,1,0:T(8,128)(2,1)S(1)}, u32[]{:S(2)}, u32[]{:S(2)}) async-start(bf16[8,144,128]{2,1,0:T(8,128)(2,1)} %broadcast_in_dim.132), calls=%async_computation.3 | async-start | bytes 589824 | tf_op jit(solution)/shard_map/all_to_all | solution.py:24
  95.9 13.5 %all-to-all-done.3 = bf16[8,144,128]{2,1,0:T(8,128)(2,1)S(1)} async-done(((bf16[8,144,128]{2,1,0:T(8,128)(2,1)}), bf16[8,144,128]{2,1,0:T(8,128)(2,1)S(1)}, u32[]{:S(2)}, u32[]{:S(2)}) %all-to-all-start.3) | async-done | bytes 294944 | tf_op jit(solution)/shard_map/all_to_all | solution.py:24
  110.0 0.2 multiply_reduce_fusion
  110.3 2.9 %fusion.9 = f32[288,512]{0,1:T(8,128)S(1)} fusion(bf16[288,2048]{1,0:T(8,128)(2,1)S(1)} %fusion.3, bf16[2048,768]{1,0:T(8,128)(2,1)} %all-gather.5.cloned.1.call-done), kind=kOutput, calls=%fused_computation.10 | convolution fusion | flops 604274688 | bytes 3866624 | tf_op jit(solution)/shard_map/dot_general | solution.py:33
  113.3 0.3 multiply_convert_fusion.3
  113.6 0.2 fusion.81
  113.8 0.3 fusion.62
  114.1 0.3 fusion.63
  114.4 0.1 fusion.14
  114.5 0.1 fusion.13
  114.8 1.8 %fusion.120 = (f32[256]{0:T(256)S(1)}, f32[256]{0:T(256)S(1)}, bf16[256,128]{0,1:T(8,128)(2,1)S(1)}) fusion(f32[128]{0:T(128)S(1)} %get-tuple-element.59, f32[288,128]{0,1:T(8,128)S(1)} %fusion.22, f32[128]{0:T(128)S(1)} %get-tuple-element.60, f32[128]{0:T(128)S(1)} %get-tuple-element.31, f32[128]{0:T(128)S(1)} %get-tuple-element.32, ...), kind=kLoop, calls=%fused_computation.283 | loop fusion | flops 2129408 | bytes 4146688 | tf_op jit(solution)/shard_map/reduce_sum | solution.py:167
  116.7 0.6 broadcast_in_dim.136
  117.3 6.8 %all-to-all-start.4 = ((f32[8,3,256]{2,1,0:T(4,128)}), f32[8,3,256]{2,1,0:T(4,128)S(1)}, u32[]{:S(2)}, u32[]{:S(2)}) async-start(f32[8,3,256]{2,1,0:T(4,128)} %broadcast_in_dim.136), calls=%async_computation.4 | async-start | bytes 65536 | tf_op jit(solution)/shard_map/all_to_all | solution.py:24
  124.2 2.1 %all-gather = bf16[512,256]{0,1:T(8,128)(2,1)} all-gather(bf16[256,256]{0,1:T(8,128)(2,1)S(1)} %pad_maximum_fusion.1), channel_id=2, replica_groups=mesh['sp_0'=8,'sp_1'=8,'fs'=4,'tp'=2] {'tp'}, dimensions={0}, use_global_device_ids=true | all-gather | bytes 393216 | tf_op jit(solution)/shard_map/all_gather | solution.py:175
  126.3 1.1 copy.92
  127.5 1.1 slice.555
  128.6 2.0 %collective-permute-start.1 = (bf16[2048,256]{1,0:T(8,128)(2,1)}, bf16[2048,256]{1,0:T(8,128)(2,1)}, u32[]{:S(2)}, u32[]{:S(2)}) collective-permute-start(bf16[2048,256]{1,0:T(8,128)(2,1)} %slice.555), channel_id=1, source_target_pairs={{0,1},{1,0},{2,3},{3,2},{4,5},{5,4},{6,7},{7,6},{8,9},{9,8},{10,11... | collective-permute-start | bytes 3145736 | tf_op jit(solution)/shard_map/ppermute | solution.py:151
  131.0 0.5 fusion.72
  131.5 1.9 %collective-permute-done.1 = bf16[2048,256]{1,0:T(8,128)(2,1)} collective-permute-done((bf16[2048,256]{1,0:T(8,128)(2,1)}, bf16[2048,256]{1,0:T(8,128)(2,1)}, u32[]{:S(2)}, u32[]{:S(2)}) %collective-permute-start.1) | collective-permute-done | bytes 1048608 | tf_op jit(solution)/shard_map/ppermute | solution.py:151
  133.4 1.7 %fusion = bf16[128,2048]{1,0:T(8,128)(2,1)S(1)} fusion(f32[128,2048]{1,0:T(8,128)S(1)} %fusion.72, bf16[2048,256]{1,0:T(8,128)(2,1)} %collective-permute-done.1, bf16[128,128]{1,0:T(8,128)(2,1)S(1)} %get-tuple-element.84, bf16[128,128]{1,0:T(8,128)(2,1)S(1)} %get-tuple-element.85), kind=kOutput, calls=%fused_computation.3 | convolution fusion | flops 134873088 | bytes 2686976 | tf_op jit(solution)/shard_map/dot_general | solution.py:33
  135.1 12.6 %all_to_all.30 = bf16[4,32,2048]{2,1,0:T(8,128)(2,1)S(1)} all-to-all(bf16[4,32,2048]{2,1,0:T(8,128)(2,1)S(1)} %bitcast.187), channel_id=1, replica_groups=mesh['sp_0'=8,'sp_1'=8,'fs'=4,'tp'=2] {'fs'}, dimensions={0} | all-to-all | bytes 1048576 | tf_op jit(solution)/shard_map/all_to_all | solution.py:186
  147.7 0.7 reduce_sum.175
  (93 shorter events, 3.2 us)
Async XLA Ops:
  6.5 39.0 %copy-start = (bf16[2048,16]{0,1:T(8,128)(2,1)S(1)}, bf16[2048,16]{0,1:T(8,128)(2,1)}, u32[]{:S(2)}) copy-start(bf16[2048,16]{0,1:T(8,128)(2,1)} %param.29) | copy-start | bytes 196612
  6.5 38.6 %copy-start.1 = (bf16[256,2048]{1,0:T(8,128)(2,1)S(1)}, bf16[256,2048]{1,0:T(8,128)(2,1)}, u32[]{:S(2)}) copy-start(bf16[256,2048]{1,0:T(8,128)(2,1)} %param.21) | copy-start | bytes 3145732
  6.5 38.6 %copy-start.6 = (f32[2048]{0:T(1024)S(1)}, f32[2048]{0:T(1024)}, u32[]{:S(2)}) copy-start(f32[2048]{0:T(1024)} %param.22) | copy-start | bytes 24580
  7.5 17.7 %collective-permute-start = (bf16[32,2048]{1,0:T(8,128)(2,1)S(1)}, bf16[32,2048]{1,0:T(8,128)(2,1)S(1)}, u32[]{:S(2)}, u32[]{:S(2)}) collective-permute-start(bf16[32,2048]{1,0:T(8,128)(2,1)S(1)} %slice.372), channel_id=1, source_target_pairs={{0,8},{8,16},{16,24},{24,32},{32,40},{40,48},{48,56},{56,64},{64,7... | collective-permute-start | bytes 393224 | tf_op jit(solution)/shard_map/ppermute | solution.py:29
  13.7 18.7 %all-to-all-start = ((bf16[8,32,768]{2,1,0:T(8,128)(2,1)}), bf16[8,32,768]{2,1,0:T(8,128)(2,1)S(1)}, u32[]{:S(2)}, u32[]{:S(2)}) async-start(bf16[8,32,768]{2,1,0:T(8,128)(2,1)} %get-tuple-element.7), calls=%async_computation | async-start | bytes 786432 | tf_op jit(solution)/shard_map/all_to_all | solution.py:102
  32.4 13.5 %copy-start.2 = (bf16[8,32,768]{2,1,0:T(8,128)(2,1)}, bf16[8,32,768]{2,1,0:T(8,128)(2,1)S(1)}, u32[]{:S(2)}) copy-start(bf16[8,32,768]{2,1,0:T(8,128)(2,1)S(1)} %all-to-all-done) | copy-start | bytes 1179652
  32.4 38.6 %all-to-all-start.1 = ((bf16[64,32,256]{2,1,0:T(8,128)(2,1)}), bf16[64,32,256]{2,1,0:T(8,128)(2,1)}, u32[]{:S(2)}, u32[]{:S(2)}) async-start(bf16[64,32,256]{2,1,0:T(8,128)(2,1)} %get-tuple-element.8), calls=%async_computation.1 | async-start | bytes 2097152 | tf_op jit(solution)/shard_map/all_to_all | solution.py:104
  45.1 0.8 copy-start.7
  45.1 0.8 copy-start.9
  45.1 65.2 %all-gather.5.cloned.1.call-start = ((), (), s32[]{:S(2)}) async-start(), calls=%async_computation.6 | async-start | bytes 3538944 | tf_op jit(solution)/shard_map/all_gather | solution.py:103
  71.0 9.3 %copy-start.5 = (f32[31,128]{1,0:T(8,128)S(1)}, f32[31,128]{1,0:T(8,128)}, u32[]{:S(2)}) copy-start(f32[31,128]{1,0:T(8,128)} %param.36) | copy-start | bytes 47620
  73.0 37.2 %copy-start.4 = (f32[2,64,128]{2,1,0:T(8,128)S(1)}, f32[2,64,128]{2,1,0:T(8,128)}, u32[]{:S(2)}) copy-start(f32[2,64,128]{2,1,0:T(8,128)} %param.41) | copy-start | bytes 196612
  74.6 15.5 %all-to-all-start.2 = ((bf16[8,144,128]{2,1,0:T(8,128)(2,1)}), bf16[8,144,128]{2,1,0:T(8,128)(2,1)S(1)}, u32[]{:S(2)}, u32[]{:S(2)}) async-start(bf16[8,144,128]{2,1,0:T(8,128)(2,1)} %broadcast_in_dim.125), calls=%async_computation.2 | async-start | bytes 589824 | tf_op jit(solution)/shard_map/all_to_all | solution.py:24
  92.2 17.2 %all-to-all-start.3 = ((bf16[8,144,128]{2,1,0:T(8,128)(2,1)}), bf16[8,144,128]{2,1,0:T(8,128)(2,1)S(1)}, u32[]{:S(2)}, u32[]{:S(2)}) async-start(bf16[8,144,128]{2,1,0:T(8,128)(2,1)} %broadcast_in_dim.132), calls=%async_computation.3 | async-start | bytes 589824 | tf_op jit(solution)/shard_map/all_to_all | solution.py:24
  114.6 9.4 %copy-start.8 = (f32[128]{0:T(128)S(1)}, f32[128]{0:T(128)}, u32[]{:S(2)}) copy-start(f32[128]{0:T(128)} %param.38) | copy-start | bytes 1540
  114.8 12.7 %copy-start.3 = (bf16[2048,768]{1,0:T(8,128)(2,1)S(1)}, bf16[2048,768]{1,0:T(8,128)(2,1)}, u32[]{:S(2)}) copy-start(bf16[2048,768]{1,0:T(8,128)(2,1)} %all-gather.5.cloned.1.call-done) | copy-start | bytes 9437188
  117.3 13.4 %all-to-all-start.4 = ((f32[8,3,256]{2,1,0:T(4,128)}), f32[8,3,256]{2,1,0:T(4,128)S(1)}, u32[]{:S(2)}, u32[]{:S(2)}) async-start(f32[8,3,256]{2,1,0:T(4,128)} %broadcast_in_dim.136), calls=%async_computation.4 | async-start | bytes 65536 | tf_op jit(solution)/shard_map/all_to_all | solution.py:24
  128.6 4.9 %collective-permute-start.1 = (bf16[2048,256]{1,0:T(8,128)(2,1)}, bf16[2048,256]{1,0:T(8,128)(2,1)}, u32[]{:S(2)}, u32[]{:S(2)}) collective-permute-start(bf16[2048,256]{1,0:T(8,128)(2,1)} %slice.555), channel_id=1, source_target_pairs={{0,1},{1,0},{2,3},{3,2},{4,5},{5,4},{6,7},{7,6},{8,9},{9,8},{10,11... | collective-permute-start | bytes 3145736 | tf_op jit(solution)/shard_map/ppermute | solution.py:151
Sparse Core Ops, SparseCore 0:
  48.0 60.3 all-gather.4

commit v3 on v2

--- a/solution.py
+++ b/solution.py
@@ -50,31 +50,22 @@
     return hi, mid, (rest - mid.astype(f32)).astype(bf16)
 
 
-def lay_out(early, late, n_all, n_y):
-    rows, ch = early[0].shape
-    ne, nl = len(early), len(late)
+VMEM = pl.BlockSpec(memory_space=pltpu.VMEM)
+
+
+def lay_out(shards, copies):
+    rows, ch = shards[0].shape
+    n = len(shards)
 
     def body(*refs):
-        ins, (first, rest) = refs[: ne + nl], refs[ne + nl :]
-        for i in range(nl):
-            w = ins[ne + i][...]
-            for k in range(n_y):
-                rest[k, :, i * ch : (i + 1) * ch] = w
-        for i in range(ne):
-            w = ins[i][...]
-            for k in range(n_all):
-                first[k, :, i * ch : (i + 1) * ch] = w
+        for i in range(n):
+            w = refs[i][...]
+            for k in range(copies):
+                refs[n][k, :, i * ch : (i + 1) * ch] = w
 
     return pl.pallas_call(
-        body,
-        out_shape=(
-            jax.ShapeDtypeStruct((n_all, rows, ne * ch), bf16),
-            jax.ShapeDtypeStruct((n_y, rows, nl * ch), bf16),
-        ),
-        in_specs=[pl.BlockSpec(memory_space=pltpu.VMEM)] * (ne + nl),
-        out_specs=(pl.BlockSpec(memory_space=pltpu.VMEM),) * 2,
-        name="lay_out",
-    )(*early, *late)
+        body, out_shape=jax.ShapeDtypeStruct((copies, rows, n * ch), bf16), in_specs=[VMEM] * n, out_specs=VMEM
+    )(*shards)
 
 
 def log_rows(logs):
@@ -93,14 +84,9 @@
     heads = step_bias.shape[0]
     p = ch // heads
     nf, nt = lax.axis_size("fs"), lax.axis_size("tp")
-    first, rest = lay_out(
-        (state_input, write_projection),
-        (state_read, mixer_gate, conv_value, conv_gate, conv_output, state_output),
-        lax.axis_size(SP),
-        lax.axis_size("sp_1"),
-    )
-    rest = lax.all_to_all(rest, "sp_1", 0, 0, tiled=True).reshape(-1, 6 * ch)
-    rest = lax.all_gather(rest, "sp_0", axis=0, tiled=True)
+    rest = lay_out((state_read, mixer_gate, conv_value, conv_gate, conv_output, state_output), 1)
+    rest = lax.all_gather(rest[0], SP, axis=0, tiled=True)
+    first = lay_out((state_input, write_projection), lax.axis_size(SP))
     first = lax.all_to_all(first, SP, 0, 0, tiled=True).reshape(-1, 2 * ch)
     halo = previous(tokens[rows - HALO :])
     normed = unit_rows(jnp.concatenate([halo, tokens], 0), norm_gain)
@@ -196,6 +182,5 @@
         P(SP, None), P(), w, w, w, w, w, w, P(), P(FT), P(FT), P(FT, SP), P(None, FT), P(None, FT), P(None, FT),
         P(None, FT), P(FT), P(FT), w, w, P(FT, None, None),
     )
-    return jax.shard_map(
-        per_device, mesh=torus, in_specs=in_specs, out_specs=P((*SP, *FT), None), check_vma=False
-    )
+
+    return jax.shard_map(per_device, mesh=torus, in_specs=in_specs, out_specs=P((*SP, *FT), None), check_vma=False)

time: 156 us -> 166 us (1.064)
  waiting for transfers between devices: 54.3 us -> 65.3 us
  starting transfers between devices: 40.8 us -> 38.8 us
    all_gather x1, waiting for transfers between devices: 0.02 us -> 27 us  [per_device(): rest = lax.all_gather(rest[0], SP, axis=0, tiled=True)]
    all_to_all x3, waiting for transfers between devices: 23.2 us -> 17.1 us  [spread(): lax.all_to_all(jnp.broadcast_to(shard[None], (n, *shard.shape)), axis, 0,...]
    all_to_all x1 -> x0, starting transfers between devices: 5.92 us -> none  [per_device(): rest = lax.all_to_all(rest, 'sp_1', 0, 0, tiled=True).reshape(-1, 6 * ch)]
    all_to_all x1 -> x0, waiting for transfers between devices: 5.56 us -> none  [per_device(): rest = lax.all_to_all(rest, 'sp_1', 0, 0, tiled=True).reshape(-1, 6 * ch)]
    all_to_all x1, waiting for transfers between devices: 23.6 us -> 19.3 us  [per_device(): first = lax.all_to_all(first, SP, 0, 0, tiled=True).reshape(-1, 2 * ch)]
    all_to_all x1, starting transfers between devices: 12.7 us -> 15.4 us  [per_device(): first = lax.all_to_all(first, SP, 0, 0, tiled=True).reshape(-1, 2 * ch)]
    pallas_call x1 -> x2, Pallas kernels: 2.11 us -> 3.41 us  [lay_out(): pl.pallas_call(body, out_shape=jax.ShapeDtypeStruct((copies, rows, n * ch...]
  transfers between devices with their start and end apart: 8 -> 7, of which waited for: 5 -> 5; matrix products, arithmetic and copies ran while one was open for 10% -> 8% of each run, Pallas kernels for 1% -> 2%
where the time goes in v3:
time: 166 us; the launch traced here: 165 us
  waiting for transfers between devices  65.3 us (39%)
  starting transfers between devices  38.8 us (23%)
  blocking collectives  17.4 us (10%)
  between operations  14.4 us (9%)
  local copies, waits for them, and re-layouts  10.1 us (6%)
  matrix products  8.03 us (5%)
  other arithmetic  7.52 us (5%)
  Pallas kernels  3.41 us (2%)
    all_gather x1, waiting for transfers between devices, per_device(): rest = lax.all_gather(rest[0], SP, axis=0, tiled=True)  27 us
    all_to_all x1, waiting for transfers between devices, per_device(): first = lax.all_to_all(first, SP, 0, 0, tiled=True).reshape(-1, 2 * ch)  19.3 us
    all_to_all x3, starting transfers between devices, spread(): lax.all_to_all(jnp.broadcast_to(shard[None], (n, *shard.shape)), axis, 0,...  17.3 us
    all_to_all x3, waiting for transfers between devices, spread(): lax.all_to_all(jnp.broadcast_to(shard[None], (n, *shard.shape)), axis, 0,...  17.1 us
    all_to_all x1, starting transfers between devices, per_device(): first = lax.all_to_all(first, SP, 0, 0, tiled=True).reshape(-1, 2 * ch)  15.4 us
    all_to_all x1, blocking collectives, per_device(): lax.all_to_all(part.astype(bf16).reshape(nf, -1, part.shape[1]), 'fs', 0,...  12.6 us
    dot_general x11, matrix products, dot(): lax.dot_general(a, b, (((ca,), (cb,)), ((), ())), preferred_element_type=...  7.66 us
    ppermute x1, starting transfers between devices, previous(): return lax.ppermute(block, SP, [(i, i + 1) for i in range(n - 1)])  4.03 us
  transfers between devices with their start and end apart: 7, of which 5 were waited for; matrix products, arithmetic and copies ran while one was open for 8% of the time, Pallas kernels for 2%

profile of v3, /device:TPU:1, one launch (start us, length us, event | category | flops | bytes accessed | tf_op | source)
XLA Modules:
  0.0 165.0 jit_solution(7458457348808763078)
XLA Ops:
  6.6 1.0 slice.372
  7.6 4.0 %collective-permute-start = (bf16[32,2048]{1,0:T(8,128)(2,1)S(1)}, bf16[32,2048]{1,0:T(8,128)(2,1)S(1)}, u32[]{:S(2)}, u32[]{:S(2)}) collective-permute-start(bf16[32,2048]{1,0:T(8,128)(2,1)S(1)} %slice.372), channel_id=1, source_target_pairs={{0,8},{8,16},{16,24},{24,32},{32,40},{40,48},{48,56},{56,64},{64,7... | collective-permute-start | bytes 393224 | tf_op jit(solution)/shard_map/ppermute | solution.py:29
  11.6 2.0 %shard_map.200 = bf16[64,32,256]{2,1,0:T(8,128)(2,1)} custom-call(bf16[32,128]{1,0:T(8,128)(2,1)} %refs_0_.3, bf16[32,128]{1,0:T(8,128)(2,1)} %refs_1_.3), custom_call_target="tpu_custom_call" | custom-call | tf_op jit(solution)/shard_map/pallas_call | solution.py:66
  13.6 15.4 %all-to-all-start = ((bf16[64,32,256]{2,1,0:T(8,128)(2,1)}), bf16[64,32,256]{2,1,0:T(8,128)(2,1)S(1)}, u32[]{:S(2)}, u32[]{:S(2)}) async-start(bf16[64,32,256]{2,1,0:T(8,128)(2,1)} %shard_map.200), calls=%async_computation | async-start | bytes 2097152 | tf_op jit(solution)/shard_map/all_to_all | solution.py:90
  29.1 1.4 shard_map.199
  30.6 0.6 slice_bitcast_fusion.17
  31.2 0.6 fusion.104
  31.8 2.7 %all-gather.3 = f32[2,1,128]{2,1,0:T(1,128)S(1)} all-gather(f32[1,1,128]{2,1,0:T(1,128)S(1)} %bitcast.210), channel_id=4, replica_groups=mesh['sp_0'=8,'sp_1'=8,'fs'=4,'tp'=2] {'tp'}, dimensions={0}, use_global_device_ids=true | all-gather | bytes 1536 | tf_op jit(solution)/shard_map/all_gather | solution.py:138
  34.6 0.3 fusion.1
  34.9 0.3 fusion.3
  35.3 0.4 fusion.15
  35.8 0.6 reduce-window.6
  36.4 0.2 slice_reduce_fusion
  36.5 0.2 reduce-window.9
  37.1 19.3 %all-to-all-done = bf16[64,32,256]{2,1,0:T(8,128)(2,1)S(1)} async-done(((bf16[64,32,256]{2,1,0:T(8,128)(2,1)}), bf16[64,32,256]{2,1,0:T(8,128)(2,1)S(1)}, u32[]{:S(2)}, u32[]{:S(2)}) %all-to-all-start) | async-done | bytes 1048608 | tf_op jit(solution)/shard_map/all_to_all | solution.py:90
  56.4 0.8 fusion.12
  57.2 0.5 divide_multiply_fusion
  57.9 0.2 convolution_convert_fusion.1
  58.0 0.8 broadcast_in_dim.125
  58.8 5.3 %all-to-all-start.1 = ((bf16[8,144,128]{2,1,0:T(8,128)(2,1)}), bf16[8,144,128]{2,1,0:T(8,128)(2,1)S(1)}, u32[]{:S(2)}, u32[]{:S(2)}) async-start(bf16[8,144,128]{2,1,0:T(8,128)(2,1)} %broadcast_in_dim.125), calls=%async_computation.1 | async-start | bytes 589824 | tf_op jit(solution)/shard_map/all_to_all | solution.py:24
  64.1 0.6 fusion.109
  64.7 0.6 slice_bitcast_fusion.47
  65.2 0.7 slice_bitcast_fusion.48
  65.9 8.0 %all-to-all-done.1 = bf16[8,144,128]{2,1,0:T(8,128)(2,1)S(1)} async-done(((bf16[8,144,128]{2,1,0:T(8,128)(2,1)}), bf16[8,144,128]{2,1,0:T(8,128)(2,1)S(1)}, u32[]{:S(2)}, u32[]{:S(2)}) %all-to-all-start.1) | async-done | bytes 294944 | tf_op jit(solution)/shard_map/all_to_all | solution.py:24
  74.9 0.3 fusion.18
  75.3 0.8 broadcast_in_dim.132
  76.0 3.4 %all-to-all-start.2 = ((bf16[8,144,128]{2,1,0:T(8,128)(2,1)}), bf16[8,144,128]{2,1,0:T(8,128)(2,1)S(1)}, u32[]{:S(2)}, u32[]{:S(2)}) async-start(bf16[8,144,128]{2,1,0:T(8,128)(2,1)} %broadcast_in_dim.132), calls=%async_computation.2 | async-start | bytes 589824 | tf_op jit(solution)/shard_map/all_to_all | solution.py:24
  79.5 0.6 slice_bitcast_fusion.5
  80.1 9.0 %all-to-all-done.2 = bf16[8,144,128]{2,1,0:T(8,128)(2,1)S(1)} async-done(((bf16[8,144,128]{2,1,0:T(8,128)(2,1)}), bf16[8,144,128]{2,1,0:T(8,128)(2,1)S(1)}, u32[]{:S(2)}, u32[]{:S(2)}) %all-to-all-start.2) | async-done | bytes 294944 | tf_op jit(solution)/shard_map/all_to_all | solution.py:24
  89.7 0.2 multiply_reduce_fusion
  90.1 27.0 %all-gather.6.cloned.1.call-done = bf16[1,2048,768]{2,1,0:T(8,128)(2,1)} async-done(((bf16[1,32,768]{2,1,0:T(8,128)(2,1)}), bf16[1,2048,768]{2,1,0:T(8,128)(2,1)}) %all-gather.6.cloned.1.call-update) | async-done | bytes 3145744 | tf_op jit(solution)/shard_map/all_gather | solution.py:88
  117.1 3.4 %fusion.9 = f32[288,512]{0,1:T(8,128)S(1)} fusion(bf16[288,2048]{1,0:T(8,128)(2,1)} %copy-done.3, bf16[2048,768]{1,0:T(8,128)(2,1)} %bitcast.188), kind=kOutput, calls=%fused_computation.10 | convolution fusion | flops 604274688 | bytes 3866624 | tf_op jit(solution)/shard_map/dot_general | solution.py:33
  120.6 1.1 slice.555
  122.0 0.3 multiply_convert_fusion.3
  122.3 0.2 fusion.81
  122.5 0.2 fusion.62
  122.7 0.3 fusion.63
  123.7 1.8 %fusion.120 = (f32[256]{0:T(256)S(1)}, f32[256]{0:T(256)S(1)}, bf16[256,128]{0,1:T(8,128)(2,1)S(1)}) fusion(f32[128]{0:T(128)S(1)} %copy-done.9, f32[288,128]{0,1:T(8,128)S(1)} %fusion.22, f32[128]{0:T(128)S(1)} %copy-done.10, f32[128]{0:T(128)S(1)} %copy-done.12, f32[128]{0:T(128)S(1)} %copy-done.13, f32[128]{0:T(128)S(1)} %copy-done.14, ...), kind=kLoop, calls=%fused_computation.283 | loop fusion | flops 2129408 | bytes 4146688 | tf_op jit(solution)/shard_map/reduce_sum | solution.py:153
  125.6 0.6 broadcast_in_dim.136
  126.2 8.6 %all-to-all-start.3 = ((f32[8,3,256]{2,1,0:T(4,128)}), f32[8,3,256]{2,1,0:T(4,128)S(1)}, u32[]{:S(2)}, u32[]{:S(2)}) async-start(f32[8,3,256]{2,1,0:T(4,128)} %broadcast_in_dim.136), calls=%async_computation.3 | async-start | bytes 65536 | tf_op jit(solution)/shard_map/all_to_all | solution.py:24
  134.9 2.1 %all-gather.1 = bf16[512,256]{0,1:T(8,128)(2,1)} all-gather(bf16[256,256]{0,1:T(8,128)(2,1)S(1)} %pad_maximum_fusion.1), channel_id=3, replica_groups=mesh['sp_0'=8,'sp_1'=8,'fs'=4,'tp'=2] {'tp'}, dimensions={0}, use_global_device_ids=true | all-gather | bytes 393216 | tf_op jit(solution)/shard_map/all_gather | solution.py:161
  137.0 1.1 copy.92
  138.2 2.1 %collective-permute-start.1 = (bf16[2048,256]{1,0:T(8,128)(2,1)}, bf16[2048,256]{1,0:T(8,128)(2,1)}, u32[]{:S(2)}, u32[]{:S(2)}) collective-permute-start(bf16[2048,256]{1,0:T(8,128)(2,1)} %slice.555), channel_id=1, source_target_pairs={{0,1},{1,0},{2,3},{3,2},{4,5},{5,4},{6,7},{7,6},{8,9},{9,8},{10,11... | collective-permute-start | bytes 3145736 | tf_op jit(solution)/shard_map/ppermute | solution.py:137
  140.7 0.5 fusion.72
  141.2 1.9 %collective-permute-done.1 = bf16[2048,256]{1,0:T(8,128)(2,1)} collective-permute-done((bf16[2048,256]{1,0:T(8,128)(2,1)}, bf16[2048,256]{1,0:T(8,128)(2,1)}, u32[]{:S(2)}, u32[]{:S(2)}) %collective-permute-start.1) | collective-permute-done | bytes 1048608 | tf_op jit(solution)/shard_map/ppermute | solution.py:137
  143.1 1.7 %fusion = bf16[128,2048]{1,0:T(8,128)(2,1)S(1)} fusion(f32[128,2048]{1,0:T(8,128)S(1)} %fusion.72, bf16[2048,256]{1,0:T(8,128)(2,1)} %collective-permute-done.1, bf16[128,128]{1,0:T(8,128)(2,1)S(1)} %get-tuple-element.80, bf16[128,128]{1,0:T(8,128)(2,1)S(1)} %get-tuple-element.81), kind=kOutput, calls=%fused_computation.3 | convolution fusion | flops 134873088 | bytes 2686976 | tf_op jit(solution)/shard_map/dot_general | solution.py:33
  144.8 12.6 %all_to_all.25 = bf16[4,32,2048]{2,1,0:T(8,128)(2,1)S(1)} all-to-all(bf16[4,32,2048]{2,1,0:T(8,128)(2,1)S(1)} %bitcast.187), channel_id=1, replica_groups=mesh['sp_0'=8,'sp_1'=8,'fs'=4,'tp'=2] {'fs'}, dimensions={0} | all-to-all | bytes 1048576 | tf_op jit(solution)/shard_map/all_to_all | solution.py:172
  157.4 0.7 reduce_sum.175
  (174 shorter events, 3.7 us)
Async XLA Ops:
  6.5 28.7 %copy-start = (bf16[2048,16]{0,1:T(8,128)(2,1)S(1)}, bf16[2048,16]{0,1:T(8,128)(2,1)}, u32[]{:S(2)}) copy-start(bf16[2048,16]{0,1:T(8,128)(2,1)} %param.29) | copy-start | bytes 196612
  6.5 28.0 %copy-start.1 = (bf16[256,2048]{1,0:T(8,128)(2,1)S(1)}, bf16[256,2048]{1,0:T(8,128)(2,1)}, u32[]{:S(2)}) copy-start(bf16[256,2048]{1,0:T(8,128)(2,1)} %param.21) | copy-start | bytes 3145732
  6.5 24.0 %copy-start.37 = (f32[4,128]{1,0:T(4,128)S(1)}, f32[4,128]{1,0:T(4,128)}, u32[]{:S(2)}) copy-start(f32[4,128]{1,0:T(4,128)} %param.35) | copy-start | bytes 6148
  6.5 25.2 %copy-start.49 = (f32[128]{0:T(128)S(1)}, f32[128]{0:T(128)}, u32[]{:S(2)}) copy-start(f32[128]{0:T(128)} %param.37) | copy-start | bytes 1540
  6.5 27.9 %copy-start.38 = (f32[4,128]{1,0:T(4,128)S(1)}, f32[4,128]{1,0:T(4,128)}, u32[]{:S(2)}) copy-start(f32[4,128]{1,0:T(4,128)} %param.33) | copy-start | bytes 6148
  6.5 27.9 %copy-start.39 = (f32[4,128]{1,0:T(4,128)S(1)}, f32[4,128]{1,0:T(4,128)}, u32[]{:S(2)}) copy-start(f32[4,128]{1,0:T(4,128)} %param.34) | copy-start | bytes 6148
  6.6 27.9 %copy-start.50 = (f32[2]{0:T(128)S(1)}, f32[2]{0:T(128)}, u32[]{:S(2)}) copy-start(f32[2]{0:T(128)} %param.31) | copy-start | bytes 28
  6.6 28.3 %copy-start.6 = (f32[2048]{0:T(1024)S(1)}, f32[2048]{0:T(1024)}, u32[]{:S(2)}) copy-start(f32[2048]{0:T(1024)} %param.22) | copy-start | bytes 24580
  7.6 26.9 %collective-permute-start = (bf16[32,2048]{1,0:T(8,128)(2,1)S(1)}, bf16[32,2048]{1,0:T(8,128)(2,1)S(1)}, u32[]{:S(2)}, u32[]{:S(2)}) collective-permute-start(bf16[32,2048]{1,0:T(8,128)(2,1)S(1)} %slice.372), channel_id=1, source_target_pairs={{0,8},{8,16},{16,24},{24,32},{32,40},{40,48},{48,56},{56,64},{64,7... | collective-permute-start | bytes 393224 | tf_op jit(solution)/shard_map/ppermute | solution.py:29
  13.6 42.8 %all-to-all-start = ((bf16[64,32,256]{2,1,0:T(8,128)(2,1)}), bf16[64,32,256]{2,1,0:T(8,128)(2,1)S(1)}, u32[]{:S(2)}, u32[]{:S(2)}) async-start(bf16[64,32,256]{2,1,0:T(8,128)(2,1)} %shard_map.200), calls=%async_computation | async-start | bytes 2097152 | tf_op jit(solution)/shard_map/all_to_all | solution.py:90
  29.0 88.1 %all-gather.6.cloned.1.call-start = ((), (), s32[]{:S(2)}) async-start(), calls=%async_computation.5 | async-start | bytes 3194880 | tf_op jit(solution)/shard_map/all_gather | solution.py:88
  31.2 3.3 %copy-start.40 = (pred[8]{0:T(512)(128)(4,1)}, pred[8]{0:T(512)(128)(4,1)S(1)}, u32[]{:S(2)}) copy-start(pred[8]{0:T(512)(128)(4,1)S(1)} %iota_compare_fusion.6) | copy-start | bytes 28
  31.2 3.3 %copy-start.47 = (pred[8]{0:T(512)(128)(4,1)}, pred[8]{0:T(512)(128)(4,1)S(1)}, u32[]{:S(2)}) copy-start(pred[8]{0:T(512)(128)(4,1)S(1)} %iota_compare_fusion.4) | copy-start | bytes 28
  35.2 22.5 %copy-start.3 = (bf16[288,2048]{1,0:T(8,128)(2,1)}, bf16[288,2048]{1,0:T(8,128)(2,1)S(1)}, u32[]{:S(2)}) copy-start(bf16[288,2048]{1,0:T(8,128)(2,1)S(1)} %fusion.3) | copy-start | bytes 3538948
  56.4 8.3 %copy-start.5 = (f32[31,128]{1,0:T(8,128)S(1)}, f32[31,128]{1,0:T(8,128)}, u32[]{:S(2)}) copy-start(f32[31,128]{1,0:T(8,128)} %param.36) | copy-start | bytes 47620
  56.4 17.9 %copy-start.41 = (pred[8]{0:T(512)(128)(4,1)S(1)}, pred[8]{0:T(512)(128)(4,1)}, u32[]{:S(2)}) copy-start(pred[8]{0:T(512)(128)(4,1)} %copy-done.40) | copy-start | bytes 28
  57.2 32.1 %copy-start.42 = (pred[8,8]{1,0:T(8,128)(4,1)S(1)}, pred[8,8]{1,0:T(8,128)(4,1)}, u32[]{:S(2)}) copy-start(pred[8,8]{1,0:T(8,128)(4,1)} %fusion.104) | copy-start | bytes 196
  57.2 32.2 %copy-start.48 = (pred[8]{0:T(512)(128)(4,1)S(1)}, pred[8]{0:T(512)(128)(4,1)}, u32[]{:S(2)}) copy-start(pred[8]{0:T(512)(128)(4,1)} %copy-done.47) | copy-start | bytes 28
  57.2 32.8 %copy-start.4 = (f32[2,64,128]{2,1,0:T(8,128)S(1)}, f32[2,64,128]{2,1,0:T(8,128)}, u32[]{:S(2)}) copy-start(f32[2,64,128]{2,1,0:T(8,128)} %param.41) | copy-start | bytes 196612
  58.8 15.1 %all-to-all-start.1 = ((bf16[8,144,128]{2,1,0:T(8,128)(2,1)}), bf16[8,144,128]{2,1,0:T(8,128)(2,1)S(1)}, u32[]{:S(2)}, u32[]{:S(2)}) async-start(bf16[8,144,128]{2,1,0:T(8,128)(2,1)} %broadcast_in_dim.125), calls=%async_computation.1 | async-start | bytes 589824 | tf_op jit(solution)/shard_map/all_to_all | solution.py:24
  76.0 13.1 %all-to-all-start.2 = ((bf16[8,144,128]{2,1,0:T(8,128)(2,1)}), bf16[8,144,128]{2,1,0:T(8,128)(2,1)S(1)}, u32[]{:S(2)}, u32[]{:S(2)}) async-start(bf16[8,144,128]{2,1,0:T(8,128)(2,1)} %broadcast_in_dim.132), calls=%async_computation.2 | async-start | bytes 589824 | tf_op jit(solution)/shard_map/all_to_all | solution.py:24
  117.1 3.4 %copy-start.2 = (bf16[1,2048,768]{2,1,0:T(8,128)(2,1)S(1)}, bf16[1,2048,768]{2,1,0:T(8,128)(2,1)}, u32[]{:S(2)}) copy-start(bf16[1,2048,768]{2,1,0:T(8,128)(2,1)} %all-gather.6.cloned.1.call-done) | copy-start | bytes 9437188
  120.6 1.9 %copy-start.44 = (f32[256]{0:T(256)S(1)}, f32[256]{0:T(256)}, u32[]{:S(2)}) copy-start(f32[256]{0:T(256)} %get-tuple-element.62) | copy-start | bytes 3076
  120.6 2.2 %copy-start.43 = (f32[256]{0:T(256)S(1)}, f32[256]{0:T(256)}, u32[]{:S(2)}) copy-start(f32[256]{0:T(256)} %get-tuple-element.63) | copy-start | bytes 3076
  121.7 1.8 %copy-start.11 = (f32[128]{0:T(128)S(1)}, f32[128]{0:T(128)}, u32[]{:S(2)}) copy-start(f32[128]{0:T(128)} %get-tuple-element.26) | copy-start | bytes 1540
  121.7 1.8 %copy-start.12 = (f32[128]{0:T(128)S(1)}, f32[128]{0:T(128)}, u32[]{:S(2)}) copy-start(f32[128]{0:T(128)} %get-tuple-element.27) | copy-start | bytes 1540
  121.7 1.8 %copy-start.13 = (f32[128]{0:T(128)S(1)}, f32[128]{0:T(128)}, u32[]{:S(2)}) copy-start(f32[128]{0:T(128)} %get-tuple-element.28) | copy-start | bytes 1540
  121.7 1.8 %copy-start.14 = (f32[128]{0:T(128)S(1)}, f32[128]{0:T(128)}, u32[]{:S(2)}) copy-start(f32[128]{0:T(128)} %get-tuple-element.29) | copy-start | bytes 1540
  121.7 1.8 %copy-start.15 = (f32[128]{0:T(128)S(1)}, f32[128]{0:T(128)}, u32[]{:S(2)}) copy-start(f32[128]{0:T(128)} %get-tuple-element.30) | copy-start | bytes 1540
  121.7 1.8 %copy-start.16 = (f32[128]{0:T(128)S(1)}, f32[128]{0:T(128)}, u32[]{:S(2)}) copy-start(f32[128]{0:T(128)} %get-tuple-element.31) | copy-start | bytes 1540
  121.7 1.8 %copy-start.17 = (f32[128]{0:T(128)S(1)}, f32[128]{0:T(128)}, u32[]{:S(2)}) copy-start(f32[128]{0:T(128)} %get-tuple-element.32) | copy-start | bytes 1540
  121.7 1.8 %copy-start.18 = (f32[128]{0:T(128)S(1)}, f32[128]{0:T(128)}, u32[]{:S(2)}) copy-start(f32[128]{0:T(128)} %get-tuple-element.33) | copy-start | bytes 1540
  121.8 1.8 %copy-start.19 = (f32[128]{0:T(128)S(1)}, f32[128]{0:T(128)}, u32[]{:S(2)}) copy-start(f32[128]{0:T(128)} %get-tuple-element.34) | copy-start | bytes 1540
  121.8 1.8 %copy-start.20 = (f32[128]{0:T(128)S(1)}, f32[128]{0:T(128)}, u32[]{:S(2)}) copy-start(f32[128]{0:T(128)} %get-tuple-element.35) | copy-start | bytes 1540
  121.8 1.8 %copy-start.21 = (f32[128]{0:T(128)S(1)}, f32[128]{0:T(128)}, u32[]{:S(2)}) copy-start(f32[128]{0:T(128)} %get-tuple-element.36) | copy-start | bytes 1540
  121.8 1.8 %copy-start.22 = (f32[128]{0:T(128)S(1)}, f32[128]{0:T(128)}, u32[]{:S(2)}) copy-start(f32[128]{0:T(128)} %get-tuple-element.37) | copy-start | bytes 1540
  121.8 1.8 %copy-start.23 = (f32[128]{0:T(128)S(1)}, f32[128]{0:T(128)}, u32[]{:S(2)}) copy-start(f32[128]{0:T(128)} %get-tuple-element.38) | copy-start | bytes 1540
  121.8 1.8 %copy-start.24 = (f32[128]{0:T(128)S(1)}, f32[128]{0:T(128)}, u32[]{:S(2)}) copy-start(f32[128]{0:T(128)} %get-tuple-element.39) | copy-start | bytes 1540
  121.8 1.8 %copy-start.25 = (f32[128]{0:T(128)S(1)}, f32[128]{0:T(128)}, u32[]{:S(2)}) copy-start(f32[128]{0:T(128)} %get-tuple-element.40) | copy-start | bytes 1540
  121.8 1.8 %copy-start.26 = (f32[128]{0:T(128)S(1)}, f32[128]{0:T(128)}, u32[]{:S(2)}) copy-start(f32[128]{0:T(128)} %get-tuple-element.41) | copy-start | bytes 1540
  121.8 1.8 %copy-start.27 = (f32[128]{0:T(128)S(1)}, f32[128]{0:T(128)}, u32[]{:S(2)}) copy-start(f32[128]{0:T(128)} %get-tuple-element.42) | copy-start | bytes 1540
  121.8 1.8 %copy-start.28 = (f32[128]{0:T(128)S(1)}, f32[128]{0:T(128)}, u32[]{:S(2)}) copy-start(f32[128]{0:T(128)} %get-tuple-element.43) | copy-start | bytes 1540
  121.9 1.8 %copy-start.29 = (f32[128]{0:T(128)S(1)}, f32[128]{0:T(128)}, u32[]{:S(2)}) copy-start(f32[128]{0:T(128)} %get-tuple-element.44) | copy-start | bytes 1540
  123.3 11.5 %copy-start.45 = (f32[128]{0:T(128)S(1)}, f32[128]{0:T(128)}, u32[]{:S(2)}) copy-start(f32[128]{0:T(128)} %param.38) | copy-start | bytes 1540
  125.5 15.0 %copy-start.30 = (f32[128]{0:T(128)S(1)}, f32[128]{0:T(128)}, u32[]{:S(2)}) copy-start(f32[128]{0:T(128)} %get-tuple-element.82) | copy-start | bytes 1540
  125.6 15.0 %copy-start.31 = (f32[128]{0:T(128)S(1)}, f32[128]{0:T(128)}, u32[]{:S(2)}) copy-start(f32[128]{0:T(128)} %get-tuple-element.83) | copy-start | bytes 1540
  126.2 14.1 %all-to-all-start.3 = ((f32[8,3,256]{2,1,0:T(4,128)}), f32[8,3,256]{2,1,0:T(4,128)S(1)}, u32[]{:S(2)}, u32[]{:S(2)}) async-start(f32[8,3,256]{2,1,0:T(4,128)} %broadcast_in_dim.136), calls=%async_computation.3 | async-start | bytes 65536 | tf_op jit(solution)/shard_map/all_to_all | solution.py:24
  138.2 4.9 %collective-permute-start.1 = (bf16[2048,256]{1,0:T(8,128)(2,1)}, bf16[2048,256]{1,0:T(8,128)(2,1)}, u32[]{:S(2)}, u32[]{:S(2)}) collective-permute-start(bf16[2048,256]{1,0:T(8,128)(2,1)} %slice.555), channel_id=1, source_target_pairs={{0,1},{1,0},{2,3},{3,2},{4,5},{5,4},{6,7},{7,6},{8,9},{9,8},{10,11... | collective-permute-start | bytes 3145736 | tf_op jit(solution)/shard_map/ppermute | solution.py:137
  (10 other events, 15.1 us)
Sparse Core Ops, SparseCore 0:
  32.8 84.2 all-gather.5

commit v4 on v3

v4 whole, which is shorter than its diff:
```python
import jax
import jax.numpy as jnp
from jax import lax
from jax.experimental import pallas as pl
from jax.experimental.pallas import tpu as pltpu
from jax.sharding import Mesh
from jax.sharding import PartitionSpec as P


C_CH = 1024
STATE = 128
D_INNER = 1024
WIDE = 31
SHORT = 4
HALO = 32
EPS = 1e-06
LOGS = 16
SP = ("sp_0", "sp_1")
FT = ("fs", "tp")
f32 = jnp.float32
bf16 = jnp.bfloat16
VMEM = pl.BlockSpec(memory_space=pltpu.VMEM)
SMEM = pl.BlockSpec(memory_space=pltpu.SMEM)
HIGHEST = lax.Precision.HIGHEST
SMALL = pltpu.CompilerParams(vmem_limit_bytes=12 * 2**20)


def dot(a, b, ca, cb, precision=None):
    return lax.dot_general(a, b, (((ca,), (cb,)), ((), ())), precision=precision, preferred_element_type=f32)


def sds(shape, dtype):
    return jax.ShapeDtypeStruct(shape, dtype)


def held(*arrays):
    return tuple(pltpu.with_memory_space_constraint(a, pltpu.VMEM) for a in arrays)


def fetched(*arrays):
    return tuple(pltpu.with_memory_space_constraint(a, pltpu.HBM) for a in arrays)


def lay_out(shards, copies):
    rows, ch = shards[0].shape
    n = len(shards)

    def body(*refs):
        for i in range(n):
            w = refs[i][...]
            for k in range(copies):
                refs[n][k, :, i * ch : (i + 1) * ch] = w

    return pl.pallas_call(
        body, out_shape=sds((copies, rows, n * ch), bf16), in_specs=[VMEM] * n, out_specs=VMEM, compiler_params=SMALL
    )(*fetched(*shards))


def in_line(mine, other, index):
    n = 2 * mine.shape[0]

    def body(at, a, b, out):
        for j, off in enumerate((0, 4, 2, 6)):
            out[pl.ds(at[0] ^ off, 1)] = a[j : j + 1]
            out[pl.ds(at[0] ^ (off + 1), 1)] = b[j : j + 1]

    return pl.pallas_call(
        body, out_shape=sds((n, *mine.shape[1:]), bf16), in_specs=[SMEM, VMEM, VMEM], out_specs=VMEM, compiler_params=SMALL, name="in_line"
    )(index, *held(mine, other))


def log_rows(logs):
    hi = logs.astype(bf16).astype(f32)
    mid = (logs - hi).astype(bf16).astype(f32)
    lo = logs - hi - mid
    row = lax.broadcasted_iota(jnp.int32, (LOGS, STATE), 0)
    return jnp.where(row == 0, hi, jnp.where(row == 1, mid, jnp.where(row == 2, lo, 0.0))).astype(bf16)


def local_states(normed, first, taps, step, left, total, copies):
    ext, _ = normed.shape
    rows, ch = step.shape

    def body(nref, wref, tref, sref, lref, logs, send, xs, w16, buf):
        buf[...] = dot(nref[...], wref[...], 1, 0).astype(bf16).astype(f32)
        at = HALO - SHORT + 1
        mix = sum(buf[at + i : at + i + rows, :] * tref[i : i + 1, :] for i in range(SHORT))
        act = jax.nn.silu(mix)
        x = act[:, :ch] * sref[...]
        w = act[:, ch:].astype(bf16)
        xs[...] = x.astype(bf16)
        w16[...] = w
        ends = dot((x * lref[...]).astype(bf16), w, 0, 0).astype(bf16)
        tail = log_rows(logs[...])
        for k in range(copies):
            send[k, :ch, :] = ends
            send[k, ch:, :] = tail

    return pl.pallas_call(
        body,
        out_shape=(sds((copies, ch + LOGS, STATE), bf16), pltpu.VMEM((rows, ch), bf16), pltpu.VMEM((rows, STATE), bf16)),
        in_specs=[VMEM] * 6,
        out_specs=(VMEM,) * 3,
        scratch_shapes=[pltpu.VMEM((ext, 2 * ch), f32)],
        compiler_params=SMALL, name="local_states",
    )(*held(normed, first, taps, step, left, total))


def spread_heads(c, heads, p):
    return jnp.concatenate([jnp.broadcast_to(c[:, h : h + 1], (p, STATE)) for h in range(heads)], 0)


def line_states(got, index, heads, p, copies):
    n, size, _ = got.shape
    ch = heads * p

    def body(at, ref, enter, before, send):
        zero = jnp.zeros((1, STATE), f32)
        acc_in, acc_all = zero, zero
        ent = jnp.zeros((ch, STATE), f32)
        tot = jnp.zeros((ch, STATE), f32)
        for k in reversed(range(n)):
            logs = jnp.sum(ref[k, ch:, :].astype(f32), axis=0, keepdims=True)
            inside = (k < at[0]).astype(f32)
            piece = ref[k, :ch, :].astype(f32)
            ent = ent + piece * spread_heads(inside * jnp.exp(acc_in), heads, p)
            tot = tot + piece * spread_heads(jnp.exp(acc_all), heads, p)
            acc_in = acc_in + inside * logs
            acc_all = acc_all + logs
        enter[...] = ent
        before[...] = jnp.broadcast_to(acc_in, (8, STATE))
        line, tail = tot.astype(bf16), log_rows(acc_all)
        for k in range(copies):
            send[k, :ch, :] = line
            send[k, ch:, :] = tail

    return pl.pallas_call(
        body,
        out_shape=(pltpu.VMEM((ch, STATE), f32), pltpu.VMEM((8, STATE), f32), sds((copies, size, STATE), bf16)),
        in_specs=[SMEM, VMEM],
        out_specs=(VMEM,) * 3,
        compiler_params=SMALL, name="line_states",
    )(index, *held(got))


def rows_done(normed, rest, got, enter, before, init, index, ftaps, ltaps, xs, w16, cum, cum_t, gain, copies):
    ext, d = normed.shape
    rows, ch = xs.shape
    n, _, _ = got.shape
    heads = cum_t.shape[0]
    p = ch // heads
    steps = 4
    kb = d // steps
    part = 64

    def body(at, nref, wref, got, enter, before, init, ftaps, ltaps, xs, w16, cum, cum_t, gain, sums, pre, back, acc, glu):
        k = pl.program_id(0)
        at_k = pl.ds(pl.multiple_of(k * kb, kb), kb)
        term = dot(nref[:, at_k], wref[:, : 4 * ch], 1, 0)
        back[at_k, :] = wref[:, 4 * ch :]

        @pl.when(k == 0)
        def _():
            acc[...] = term

        @pl.when(k > 0)
        def _():
            acc[...] += term

        @pl.when(k == steps - 1)
        def _():
            glu[...] = acc[:, 2 * ch : 3 * ch].astype(bf16).astype(f32) * jax.nn.sigmoid(
                acc[:, 3 * ch :].astype(bf16).astype(f32)
            )
            acc[:, : 2 * ch] = acc[:, : 2 * ch].astype(bf16).astype(f32)
            s_at, l_at = HALO - SHORT + 1, HALO - WIDE + 1
            read = sum(acc[s_at + i : s_at + i + rows, :ch] * ftaps[i : i + 1, :] for i in range(SHORT))
            read = jax.nn.silu(read).astype(bf16)
            z = jax.nn.silu(acc[HALO:, ch : 2 * ch])
            acc_in = jnp.zeros((1, STATE), f32)
            start = enter[...]
            b = before[0:1, :]
            for j in reversed(range(n)):
                logs = jnp.sum(got[j, ch:, :].astype(f32), axis=0, keepdims=True)
                inside = (j < at[0]).astype(f32)
                start = start + got[j, :ch, :].astype(f32) * spread_heads(inside * jnp.exp(acc_in + b), heads, p)
                acc_in = acc_in + inside * logs
            start = start + init[...] * spread_heads(jnp.exp(acc_in + b), heads, p)
            y = dot(read, start.astype(bf16), 1, 1) * jnp.exp(cum[...])
            scores = dot(read, w16[...], 1, 1)
            lower = lax.broadcasted_iota(jnp.int32, (rows, rows), 0) >= lax.broadcasted_iota(jnp.int32, (rows, rows), 1)
            lane = lax.broadcasted_iota(jnp.int32, (rows, ch), 1)
            for h in range(heads):
                gap = jnp.where(lower, cum[:, h * p : h * p + 1] - cum_t[h : h + 1, :], 0.0)
                m = jnp.where(lower, jnp.exp(gap) * scores, 0.0).astype(bf16)
                x = jnp.where(lane // p == h, xs[...].astype(f32), 0.0).astype(bf16)
                y = y + dot(m, x, 1, 0)
            gated = y * z
            mix = jnp.concatenate(
                [
                    sum(glu[l_at + r + i : l_at + r + i + part, :] * ltaps[i : i + 1, :] for i in range(WIDE))
                    for r in range(0, rows, part)
                ],
                0,
            )
            squares = jnp.concatenate([mix, mix * mix, gated * gated], 1)
            pick = lax.broadcasted_iota(jnp.int32, (8, 3 * ch), 1) // ch == lax.broadcasted_iota(jnp.int32, (8, 3 * ch), 0)
            found = dot(jnp.where(pick, 1.0, 0.0), squares, 1, 1, HIGHEST)
            for j in range(copies):
                sums[j] = found[:3]
            pre[:, :ch] = mix.astype(bf16)
            pre[:, ch:] = (gated * gain[...]).astype(bf16)

    small = (got, enter, before, init, ftaps, ltaps, xs, w16, cum, cum_t, gain)
    return pl.pallas_call(
        body,
        grid=(steps,),
        out_shape=(sds((copies, 3, rows), f32), pltpu.VMEM((rows, 2 * ch), bf16), pltpu.VMEM((d, 2 * ch), bf16)),
        in_specs=[SMEM, VMEM, pl.BlockSpec((kb, 6 * ch), lambda k: (k, 0)), *[VMEM] * len(small)],
        out_specs=(pl.BlockSpec((copies, 3, rows), lambda k: (0, 0, 0)), VMEM, VMEM),
        scratch_shapes=[pltpu.VMEM((ext, 4 * ch), f32), pltpu.VMEM((ext, ch), f32)],
        compiler_params=SMALL, name="rows_done",
    )(index, *held(normed), *fetched(rest), *held(*small))


def output_rows(sums, both, gains, own, other, index, nf, nt):
    copies, _, rows = sums.shape
    ch = gains.shape[1]
    d = own.shape[0]
    piece = rows // (nf * nt)

    def body(at, sref, bref, gref, wa, wb, out, cols, act):
        tp = at[0]
        s = sref[0]
        for j in range(1, copies):
            s = s + sref[j]
        cols[...] = jnp.transpose(jnp.concatenate([s, jnp.zeros((5, rows), f32)], 0))
        for i in range(nf):
            at_row = pl.multiple_of(i * (nt * piece) + tp * piece, piece)
            here = slice(i * piece, (i + 1) * piece)
            t = cols[pl.ds(at_row, piece), :]
            mean = t[:, 0:1] / C_CH
            rstd = lax.rsqrt(t[:, 1:2] / C_CH - mean * mean + EPS)
            scale = lax.rsqrt(t[:, 2:3] / D_INNER + EPS)
            for j in range(nt):
                src = tp if j == 0 else 1 - tp
                a = bref[pl.ds(pl.multiple_of(src * rows + at_row, piece), piece), :].astype(f32)
                conv = jax.nn.silu((a[:, :ch] - mean) * rstd * gref[pl.ds(src, 1), :])
                act[here, 2 * j * ch : (2 * j + 1) * ch] = conv.astype(bf16)
                act[here, (2 * j + 1) * ch : (2 * j + 2) * ch] = (a[:, ch:] * scale).astype(bf16)
        term = dot(act[:, : 2 * ch], wa[...], 1, 1) + dot(act[:, 2 * ch :], wb[...], 1, 1)
        out[...] = term.astype(bf16).reshape(nf, piece, d)

    return pl.pallas_call(
        body,
        out_shape=sds((nf, piece, d), bf16),
        in_specs=[SMEM, *[VMEM] * 5],
        out_specs=VMEM,
        scratch_shapes=[pltpu.VMEM((rows, 8), f32), pltpu.VMEM((nf * piece, 4 * ch), bf16)],
        compiler_params=SMALL, name="output_rows",
    )(index, *held(sums, both, gains, own, other))


def per_device(
    tokens, norm_gain, conv_value, conv_gate, mixer_gate, state_input, write_projection, state_read,
    step_proj, step_bias, decay_log, decay_extra, input_taps, write_taps, fetch_taps, long_taps,
    conv_gain, state_gain, conv_output, state_output, initial_state,
):
    rows = tokens.shape[0]
    ch = conv_value.shape[1]
    heads = step_bias.shape[0]
    p = ch // heads
    nf, nt = lax.axis_size("fs"), lax.axis_size("tp")
    iz, iy, tp = (lax.axis_index(a).astype(jnp.int32).reshape(1) for a in ("sp_0", "sp_1", "tp"))
    ny = lax.axis_size("sp_1")
    block = lay_out((state_read, mixer_gate, conv_value, conv_gate, conv_output, state_output), 1)
    for bit in (4, 2):
        block = jnp.concatenate([block, lax.ppermute(block, "sp_1", [(i, i ^ bit) for i in range(ny)])], 0)
    other = lax.ppermute(block, "sp_1", [(i, i ^ 1) for i in range(ny)])
    rest = in_line(block, other, iy).reshape(-1, 6 * ch)
    rest = lax.all_gather(rest, "sp_0", axis=0, tiled=True)
    first = lay_out((state_input, write_projection), lax.axis_size(SP))
    first = lax.all_to_all(first, SP, 0, 0, tiled=True).reshape(-1, 2 * ch)
    n = lax.axis_size(SP)
    halo = lax.ppermute(tokens[rows - HALO :], SP, [(i, i + 1) for i in range(n - 1)])
    v = jnp.concatenate([halo, tokens], 0).astype(f32)
    normed = (v * lax.rsqrt(jnp.mean(v * v, axis=1, keepdims=True) + EPS) * norm_gain).astype(bf16)
    step_all = jnp.dot(normed[HALO:], step_proj, preferred_element_type=f32)
    me = lax.axis_index("fs") * nt + lax.axis_index("tp")
    step = jax.nn.softplus(lax.dynamic_slice_in_dim(step_all, me * heads, heads, 1) + step_bias)
    log_step = (-jnp.exp(decay_log) * step + decay_extra.T).T
    cum_t = jnp.cumsum(log_step, axis=1)
    total = cum_t[:, -1]
    cum = jnp.repeat(cum_t.T, p, axis=1)
    step = jnp.repeat(step, p, axis=1)
    left = jnp.repeat(jnp.exp(total[:, None] - cum_t).T, p, axis=1)
    total = jnp.pad(total[None], ((0, 0), (0, STATE - heads)))
    gains = lax.all_gather(conv_gain, "tp")
    taps = jnp.concatenate([input_taps, write_taps], 1)
    send, xs, w16 = local_states(normed, first, taps, step, left, total, ny)
    got = lax.all_to_all(send, "sp_1", 0, 0, tiled=True)
    enter, before, send = line_states(got, iy, heads, p, lax.axis_size("sp_0"))
    got = lax.all_to_all(send, "sp_0", 0, 0, tiled=True)
    sums, pre, back = rows_done(
        normed, rest, got, enter, before, initial_state.reshape(ch, STATE), iz, fetch_taps, long_taps, xs, w16,
        cum, cum_t, state_gain[None], nf * nt,
    )
    sums = lax.all_to_all(sums, FT, 0, 0, tiled=True)
    both = lax.all_gather(pre, "tp", axis=0, tiled=True)
    back_other = lax.ppermute(back, "tp", [(i, nt - 1 - i) for i in range(nt)])
    out = output_rows(sums, both, gains, back, back_other, tp, nf, nt)
    pieces = lax.all_to_all(out, "fs", 0, 0, tiled=True)
    return jnp.sum(pieces.astype(f32), 0).astype(bf16)


def solution(mesh):
    torus = Mesh(
        mesh.devices.reshape(8, 8, mesh.shape["fs"], mesh.shape["tp"]), ("sp_0", "sp_1", "fs", "tp")
    )
    w = P(SP, FT)
    in_specs = (
        P(SP, None), P(), w, w, w, w, w, w, P(), P(FT), P(FT), P(FT, SP), P(None, FT), P(None, FT), P(None, FT),
        P(None, FT), P(FT), P(FT), w, w, P(FT, None, None),
    )

    return jax.shard_map(per_device, mesh=torus, in_specs=in_specs, out_specs=P((*SP, *FT), None), check_vma=False)
```

time: 166 us -> 159 us (0.958)
  waiting for transfers between devices: 65.3 us -> 43.3 us
  blocking collectives: 17.4 us -> 34.4 us
  starting transfers between devices: 38.8 us -> 48.2 us
  local copies, waits for them, and re-layouts: 10.1 us -> 1.67 us
  Pallas kernels: 3.41 us -> 11.7 us
  matrix products: 8.03 us -> 0.37 us
  other arithmetic: 7.52 us -> 4.94 us
    all_gather x1, waiting for transfers between devices: 27 us -> 0.01 us  [per_device(): rest = lax.all_gather(rest, 'sp_0', axis=0, tiled=True)]
    all_to_all x1 -> x2, blocking collectives: 12.6 us -> 30.2 us  [the longest x1 19.2 us: per_device(): got = lax.all_to_all(send, 'sp_1', 0, 0, tiled=True)]
    ppermute x1 -> x4, starting transfers between devices: 4.03 us -> 16.6 us  [the longest x2 12.8 us: per_device(): lax.ppermute(block, 'sp_1', [(i, i ^ bit) for i in range(ny)])]
    ppermute x1 -> x4, waiting for transfers between devices: 0.01 us -> 9.85 us  [the longest x1 5.29 us: per_device(): other = lax.ppermute(block, 'sp_1', [(i, i ^ 1) for i in range(ny)])]
    all_to_all x3 -> x2, starting transfers between devices: 17.3 us -> 8.14 us  [the longest x1 4.72 us: per_device(): sums = lax.all_to_all(sums, FT, 0, 0, tiled=True)]
    pallas_call x2 -> x7, Pallas kernels: 3.41 us -> 11.7 us  [the longest x1 5.23 us: rows_done(): pl.pallas_call(body, grid=(steps,), out_shape=(sds((copies, 3, rows), f32...]
    dot_general x12 -> x1, matrix products: 8.03 us -> 0.37 us  [per_device(): step_all = jnp.dot(normed[HALO:], step_proj, preferred_element_type=f32)]
    all_to_all x3 -> x2, waiting for transfers between devices: 17.1 us -> 12.9 us  [the longest x1 10.2 us: per_device(): got = lax.all_to_all(send, 'sp_0', 0, 0, tiled=True)]
  transfers between devices with their start and end apart: 7 -> 9, of which waited for: 5 -> 6; matrix products, arithmetic and copies ran while one was open for 8% -> 4% of each run, Pallas kernels for 2% -> 2%
where the time goes in v4:
time: 159 us; the launch traced here: 158 us
  starting transfers between devices  48.2 us (30%)
  waiting for transfers between devices  43.3 us (27%)
  blocking collectives  34.4 us (22%)
  between operations  13.8 us (9%)
  Pallas kernels  11.7 us (7%)
  other arithmetic  4.94 us (3%)
  local copies, waits for them, and re-layouts  1.67 us (1%)
    all_to_all x1, waiting for transfers between devices, per_device(): first = lax.all_to_all(first, SP, 0, 0, tiled=True).reshape(-1, 2 * ch)  20.6 us
    all_to_all x1, blocking collectives, per_device(): got = lax.all_to_all(send, 'sp_1', 0, 0, tiled=True)  19.2 us
    all_to_all x1, starting transfers between devices, per_device(): first = lax.all_to_all(first, SP, 0, 0, tiled=True).reshape(-1, 2 * ch)  17.8 us
    ppermute x2, starting transfers between devices, per_device(): lax.ppermute(block, 'sp_1', [(i, i ^ bit) for i in range(ny)])  12.8 us
    all_to_all x1, blocking collectives, per_device(): pieces = lax.all_to_all(out, 'fs', 0, 0, tiled=True)  10.9 us
    all_to_all x1, waiting for transfers between devices, per_device(): got = lax.all_to_all(send, 'sp_0', 0, 0, tiled=True)  10.2 us
    ppermute x1, starting transfers between devices, per_device(): back_other = lax.ppermute(back, 'tp', [(i, nt - 1 - i) for i in range(nt)])  5.63 us
    ppermute x1, waiting for transfers between devices, per_device(): other = lax.ppermute(block, 'sp_1', [(i, i ^ 1) for i in range(ny)])  5.29 us
  transfers between devices with their start and end apart: 9, of which 6 were waited for; matrix products, arithmetic and copies ran while one was open for 4% of the time, Pallas kernels for 2%

profile of v4, /device:TPU:1, one launch (start us, length us, event | category | flops | bytes accessed | tf_op | source)
XLA Modules:
  0.0 158.4 jit_solution(16163846873369471209)
XLA Ops:
  6.5 0.8 shard_map.199
  7.4 8.3 %collective-permute-start.1 = (bf16[1,32,768]{2,1,0:T(8,128)(2,1)S(1)}, bf16[1,32,768]{2,1,0:T(8,128)(2,1)S(1)}, u32[]{:S(2)}, u32[]{:S(2)}) collective-permute-start(bf16[1,32,768]{2,1,0:T(8,128)(2,1)S(1)} %shard_map.199), channel_id=1, source_target_pairs={{0,32},{8,40},{16,48},{24,56},{32,0},{40,8},{48,16},{56,24},{1,33}... | collective-permute-start | bytes 147464 | tf_op jit(solution)/shard_map/ppermute | solution.py:278
  15.6 1.5 collective-permute-done.1
  17.2 4.6 %collective-permute-start.2 = (bf16[2,32,768]{2,1,0:T(8,128)(2,1)S(1)}, bf16[2,32,768]{2,1,0:T(8,128)(2,1)S(1)}, u32[]{:S(2)}, u32[]{:S(2)}) collective-permute-start(bf16[2,32,768]{2,1,0:T(8,128)(2,1)S(1)} %pad_maximum_fusion.2), channel_id=1, source_target_pairs={{0,16},{8,24},{16,0},{24,8},{32,48},{40,56},{48,32},{56,40},{1,17}... | collective-permute-start | bytes 294920 | tf_op jit(solution)/shard_map/ppermute | solution.py:278
  21.7 3.0 %collective-permute-done.2 = bf16[2,32,768]{2,1,0:T(8,128)(2,1)S(1)} collective-permute-done((bf16[2,32,768]{2,1,0:T(8,128)(2,1)S(1)}, bf16[2,32,768]{2,1,0:T(8,128)(2,1)S(1)}, u32[]{:S(2)}, u32[]{:S(2)}) %collective-permute-start.2) | collective-permute-done | bytes 98336 | tf_op jit(solution)/shard_map/ppermute | solution.py:278
  24.8 0.0 copy-start.10
  24.9 2.3 %collective-permute-start.3 = (bf16[4,32,768]{2,1,0:T(8,128)(2,1)S(1)}, bf16[4,32,768]{2,1,0:T(8,128)(2,1)S(1)}, u32[]{:S(2)}, u32[]{:S(2)}) collective-permute-start(bf16[4,32,768]{2,1,0:T(8,128)(2,1)S(1)} %pad_maximum_fusion.1.a), channel_id=1, source_target_pairs={{0,8},{8,0},{16,24},{24,16},{32,40},{40,32},{48,56},{56,48},{1,9},... | collective-permute-start | bytes 589832 | tf_op jit(solution)/shard_map/ppermute | solution.py:279
  27.2 5.3 %collective-permute-done.3.b = bf16[4,32,768]{2,1,0:T(8,128)(2,1)S(1)} collective-permute-done((bf16[4,32,768]{2,1,0:T(8,128)(2,1)S(1)}, bf16[4,32,768]{2,1,0:T(8,128)(2,1)S(1)}, u32[]{:S(2)}, u32[]{:S(2)}) %collective-permute-start.3) | collective-permute-done | bytes 196640 | tf_op jit(solution)/shard_map/ppermute | solution.py:279
  32.5 0.8 in_line.1
  33.3 0.0 all-gather.4.cloned.1.call-update
  33.3 0.9 slice.15
  34.2 1.5 collective-permute-start
  35.7 2.0 %shard_map.200 = bf16[64,32,256]{2,1,0:T(8,128)(2,1)} custom-call(bf16[32,128]{1,0:T(8,128)(2,1)} %refs_0_.3, bf16[32,128]{1,0:T(8,128)(2,1)} %refs_1_.3), custom_call_target="tpu_custom_call" | custom-call | tf_op jit(solution)/shard_map/pallas_call | solution.py:54
  37.7 17.8 %all-to-all-start = ((bf16[64,32,256]{2,1,0:T(8,128)(2,1)}), bf16[64,32,256]{2,1,0:T(8,128)(2,1)S(1)}, u32[]{:S(2)}, u32[]{:S(2)}) async-start(bf16[64,32,256]{2,1,0:T(8,128)(2,1)} %shard_map.200), calls=%async_computation | async-start | bytes 2097152 | tf_op jit(solution)/shard_map/all_to_all | solution.py:283
  55.5 0.0 copy-start.6
  55.6 0.0 copy-start.9
  55.6 1.5 fusion
  57.1 1.6 fusion.2.nref
  58.7 0.4 fusion.3
  59.1 0.0 copy-done.9
  59.1 0.1 fusion.5
  59.2 0.6 reduce-window.6
  59.9 0.2 slice_reduce_fusion
  60.0 0.2 reduce-window.9
  60.2 0.1 add_bitcast_fusion
  60.3 0.2 slice_reduce_fusion.1
  60.5 0.1 exponential_bitcast_fusion
  60.6 0.1 copy.31.lref
  60.7 0.0 copy-start.1
  60.7 0.0 copy-start.4
  60.7 0.1 copy.30.sref
  60.8 20.6 %all-to-all-done = bf16[64,32,256]{2,1,0:T(8,128)(2,1)S(1)} async-done(((bf16[64,32,256]{2,1,0:T(8,128)(2,1)}), bf16[64,32,256]{2,1,0:T(8,128)(2,1)S(1)}, u32[]{:S(2)}, u32[]{:S(2)}) %all-to-all-start) | async-done | bytes 1048608 | tf_op jit(solution)/shard_map/all_to_all | solution.py:283
  81.4 0.9 local_states.1
  82.4 19.2 %all_to_all.25.ref = bf16[8,144,128]{2,1,0:T(8,128)(2,1)S(1)} all-to-all(bf16[8,144,128]{2,1,0:T(8,128)(2,1)S(1)} %get-tuple-element.14), channel_id=1, replica_groups=mesh['sp_0'=8,'sp_1'=8,'fs'=4,'tp'=2] {'sp_1'}, dimensions={0} | all-to-all | bytes 589824 | tf_op jit(solution)/shard_map/all_to_all | solution.py:301
  101.6 0.9 line_states.1
  102.5 3.4 %all-to-all-start.2 = ((bf16[8,144,128]{2,1,0:T(8,128)(2,1)}), bf16[8,144,128]{2,1,0:T(8,128)(2,1)S(1)}, u32[]{:S(2)}, u32[]{:S(2)}) async-start(bf16[8,144,128]{2,1,0:T(8,128)(2,1)} %get-tuple-element.15), calls=%async_computation.2 | async-start | bytes 589824 | tf_op jit(solution)/shard_map/all_to_all | solution.py:303
  105.9 0.1 copy.32.cum
  106.0 10.2 %all-to-all-done.2.got = bf16[8,144,128]{2,1,0:T(8,128)(2,1)S(1)} async-done(((bf16[8,144,128]{2,1,0:T(8,128)(2,1)}), bf16[8,144,128]{2,1,0:T(8,128)(2,1)S(1)}, u32[]{:S(2)}, u32[]{:S(2)}) %all-to-all-start.2) | async-done | bytes 294944 | tf_op jit(solution)/shard_map/all_to_all | solution.py:303
  116.2 0.0 copy-start.11
  116.2 5.2 %rows_done.1 = (f32[8,3,256]{2,1,0:T(4,128)}, bf16[256,256]{1,0:T(8,128)(2,1)S(1)}, bf16[2048,256]{1,0:T(8,128)(2,1)S(1)}) custom-call(s32[1]{0:T(128)} %bitcast.1.at, bf16[288,2048]{1,0:T(8,128)(2,1)S(1)} %fusion.2.nref, bf16[2048,768]{1,0:T(8,128)(2,1)} %all-gather.4.cloned.1.call-done.wref, bf16[8,144,128]{2,1,0:T(8,128)(2,1)S(1)} %all-to-all-done.2.got, ...), custom_call_target="tpu_custom_call" | custom-call | tf_op jit(solution)/shard_map/rows_done/pallas_call | solution.py:215
  121.4 5.6 %collective-permute-start.4 = (bf16[2048,256]{1,0:T(8,128)(2,1)S(1)}, bf16[2048,256]{1,0:T(8,128)(2,1)S(1)}, u32[]{:S(2)}, u32[]{:S(2)}) collective-permute-start(bf16[2048,256]{1,0:T(8,128)(2,1)S(1)} %get-tuple-element.22.wa), channel_id=1, source_target_pairs={{0,1},{1,0},{2,3},{3,2},{4,5},{5,4},{6,7},{7,6},{8,9},{9,8},{10,11... | collective-permute-start | bytes 3145736 | tf_op jit(solution)/shard_map/ppermute | solution.py:310
  127.1 2.3 %all-gather.1 = f32[2,1,128]{2,1,0:T(1,128)S(1)} all-gather(f32[1,1,128]{2,1,0:T(1,128)S(1)} %bitcast.47), channel_id=2, replica_groups=mesh['sp_0'=8,'sp_1'=8,'fs'=4,'tp'=2] {'tp'}, dimensions={0}, use_global_device_ids=true | all-gather | bytes 1536 | tf_op jit(solution)/shard_map/all_gather | solution.py:298
  129.3 4.7 %all-to-all-start.3 = ((f32[8,3,256]{2,1,0:T(4,128)}), f32[8,3,256]{2,1,0:T(4,128)S(1)}, u32[]{:S(2)}, u32[]{:S(2)}) async-start(f32[8,3,256]{2,1,0:T(4,128)} %get-tuple-element.20), calls=%async_computation.3 | async-start | bytes 65536 | tf_op jit(solution)/shard_map/all_to_all | solution.py:308
  134.0 2.0 %all_gather.13.bref = bf16[512,256]{1,0:T(8,128)(2,1)S(1)} all-gather(bf16[256,256]{1,0:T(8,128)(2,1)S(1)} %get-tuple-element.21), channel_id=1, replica_groups=mesh['sp_0'=8,'sp_1'=8,'fs'=4,'tp'=2] {'tp'}, dimensions={0}, use_global_device_ids=true | all-gather | bytes 393216 | tf_op jit(solution)/shard_map/all_gather | solution.py:309
  136.0 2.7 %all-to-all-done.3.sref = f32[8,3,256]{2,1,0:T(4,128)S(1)} async-done(((f32[8,3,256]{2,1,0:T(4,128)}), f32[8,3,256]{2,1,0:T(4,128)S(1)}, u32[]{:S(2)}, u32[]{:S(2)}) %all-to-all-start.3) | async-done | bytes 24608 | tf_op jit(solution)/shard_map/all_to_all | solution.py:308
  138.8 1.1 output_rows.1
  139.8 10.9 %all_to_all.26 = bf16[4,32,2048]{2,1,0:T(8,128)(2,1)S(1)} all-to-all(bf16[4,32,2048]{2,1,0:T(8,128)(2,1)S(1)} %output_rows.1), channel_id=1, replica_groups=mesh['sp_0'=8,'sp_1'=8,'fs'=4,'tp'=2] {'fs'}, dimensions={0} | all-to-all | bytes 1048576 | tf_op jit(solution)/shard_map/all_to_all | solution.py:312
  150.8 0.7 reduce_sum.22
  (32 shorter events, 0.2 us)
Async XLA Ops:
  6.5 52.2 %copy-start = (bf16[2048,16]{0,1:T(8,128)(2,1)S(1)}, bf16[2048,16]{0,1:T(8,128)(2,1)}, u32[]{:S(2)}) copy-start(bf16[2048,16]{0,1:T(8,128)(2,1)} %param.29) | copy-start | bytes 196612
  6.5 109.6 %all-gather.4.cloned.1.call-start = ((), (), s32[]{:S(2)}) async-start(), calls=%async_computation.5 | async-start | bytes 3538944 | tf_op jit(solution)/shard_map/all_gather | solution.py:281
  7.4 9.8 %collective-permute-start.1 = (bf16[1,32,768]{2,1,0:T(8,128)(2,1)S(1)}, bf16[1,32,768]{2,1,0:T(8,128)(2,1)S(1)}, u32[]{:S(2)}, u32[]{:S(2)}) collective-permute-start(bf16[1,32,768]{2,1,0:T(8,128)(2,1)S(1)} %shard_map.199), channel_id=1, source_target_pairs={{0,32},{8,40},{16,48},{24,56},{32,0},{40,8},{48,16},{56,24},{1,33}... | collective-permute-start | bytes 147464 | tf_op jit(solution)/shard_map/ppermute | solution.py:278
  17.2 7.6 %collective-permute-start.2 = (bf16[2,32,768]{2,1,0:T(8,128)(2,1)S(1)}, bf16[2,32,768]{2,1,0:T(8,128)(2,1)S(1)}, u32[]{:S(2)}, u32[]{:S(2)}) collective-permute-start(bf16[2,32,768]{2,1,0:T(8,128)(2,1)S(1)} %pad_maximum_fusion.2), channel_id=1, source_target_pairs={{0,16},{8,24},{16,0},{24,8},{32,48},{40,56},{48,32},{56,40},{1,17}... | collective-permute-start | bytes 294920 | tf_op jit(solution)/shard_map/ppermute | solution.py:278
  24.8 30.7 %copy-start.10 = (f32[2]{0:T(128)S(1)}, f32[2]{0:T(128)}, u32[]{:S(2)}) copy-start(f32[2]{0:T(128)} %param.31) | copy-start | bytes 28
  24.8 30.7 %copy-start.7 = (f32[4,128]{1,0:T(4,128)S(1)}, f32[4,128]{1,0:T(4,128)}, u32[]{:S(2)}) copy-start(f32[4,128]{1,0:T(4,128)} %param.34) | copy-start | bytes 6148
  24.8 30.7 %copy-start.8 = (f32[4,128]{1,0:T(4,128)S(1)}, f32[4,128]{1,0:T(4,128)}, u32[]{:S(2)}) copy-start(f32[4,128]{1,0:T(4,128)} %param.33) | copy-start | bytes 6148
  24.9 7.6 %collective-permute-start.3 = (bf16[4,32,768]{2,1,0:T(8,128)(2,1)S(1)}, bf16[4,32,768]{2,1,0:T(8,128)(2,1)S(1)}, u32[]{:S(2)}, u32[]{:S(2)}) collective-permute-start(bf16[4,32,768]{2,1,0:T(8,128)(2,1)S(1)} %pad_maximum_fusion.1.a), channel_id=1, source_target_pairs={{0,8},{8,0},{16,24},{24,16},{32,40},{40,32},{48,56},{56,48},{1,9},... | collective-permute-start | bytes 589832 | tf_op jit(solution)/shard_map/ppermute | solution.py:279
  33.3 23.9 %copy-start.5 = (f32[2048]{0:T(1024)S(1)}, f32[2048]{0:T(1024)}, u32[]{:S(2)}) copy-start(f32[2048]{0:T(1024)} %param.22) | copy-start | bytes 24580
  34.2 21.4 %collective-permute-start = (bf16[32,2048]{1,0:T(8,128)(2,1)S(1)}, bf16[32,2048]{1,0:T(8,128)(2,1)S(1)}, u32[]{:S(2)}, u32[]{:S(2)}) collective-permute-start(bf16[32,2048]{1,0:T(8,128)(2,1)S(1)} %slice.15), channel_id=1, source_target_pairs={{0,8},{8,16},{16,24},{24,32},{32,40},{40,48},{48,56},{56,64},{64,7... | collective-permute-start | bytes 393224 | tf_op jit(solution)/shard_map/ppermute | solution.py:285
  37.7 43.8 %all-to-all-start = ((bf16[64,32,256]{2,1,0:T(8,128)(2,1)}), bf16[64,32,256]{2,1,0:T(8,128)(2,1)S(1)}, u32[]{:S(2)}, u32[]{:S(2)}) async-start(bf16[64,32,256]{2,1,0:T(8,128)(2,1)} %shard_map.200), calls=%async_computation | async-start | bytes 2097152 | tf_op jit(solution)/shard_map/all_to_all | solution.py:283
  55.5 3.6 %copy-start.6 = (f32[2,256]{1,0:T(2,128)S(1)}, f32[2,256]{1,0:T(2,128)}, u32[]{:S(2)}) copy-start(f32[2,256]{1,0:T(2,128)} %param.32) | copy-start | bytes 6148
  55.6 3.6 %copy-start.9 = (f32[2]{0:T(128)S(1)}, f32[2]{0:T(128)}, u32[]{:S(2)}) copy-start(f32[2]{0:T(128)} %param.30) | copy-start | bytes 28
  60.7 55.5 %copy-start.1 = (f32[2,64,128]{2,1,0:T(8,128)S(1)}, f32[2,64,128]{2,1,0:T(8,128)}, u32[]{:S(2)}) copy-start(f32[2,64,128]{2,1,0:T(8,128)} %param.41) | copy-start | bytes 196612
  60.7 55.5 %copy-start.2 = (f32[31,128]{1,0:T(8,128)S(1)}, f32[31,128]{1,0:T(8,128)}, u32[]{:S(2)}) copy-start(f32[31,128]{1,0:T(8,128)} %ltaps.1) | copy-start | bytes 47620
  60.7 55.5 %copy-start.3 = (f32[4,128]{1,0:T(4,128)S(1)}, f32[4,128]{1,0:T(4,128)}, u32[]{:S(2)}) copy-start(f32[4,128]{1,0:T(4,128)} %ftaps.1) | copy-start | bytes 6148
  60.7 55.4 %copy-start.4 = (f32[128]{0:T(128)S(1)}, f32[128]{0:T(128)}, u32[]{:S(2)}) copy-start(f32[128]{0:T(128)} %param.38) | copy-start | bytes 1540
  102.5 13.7 %all-to-all-start.2 = ((bf16[8,144,128]{2,1,0:T(8,128)(2,1)}), bf16[8,144,128]{2,1,0:T(8,128)(2,1)S(1)}, u32[]{:S(2)}, u32[]{:S(2)}) async-start(bf16[8,144,128]{2,1,0:T(8,128)(2,1)} %get-tuple-element.15), calls=%async_computation.2 | async-start | bytes 589824 | tf_op jit(solution)/shard_map/all_to_all | solution.py:303
  116.2 10.9 %copy-start.11 = (f32[128]{0:T(128)S(1)}, f32[128]{0:T(128)}, u32[]{:S(2)}) copy-start(f32[128]{0:T(128)} %param.37) | copy-start | bytes 1540
  121.4 17.3 %collective-permute-start.4 = (bf16[2048,256]{1,0:T(8,128)(2,1)S(1)}, bf16[2048,256]{1,0:T(8,128)(2,1)S(1)}, u32[]{:S(2)}, u32[]{:S(2)}) collective-permute-start(bf16[2048,256]{1,0:T(8,128)(2,1)S(1)} %get-tuple-element.22.wa), channel_id=1, source_target_pairs={{0,1},{1,0},{2,3},{3,2},{4,5},{5,4},{6,7},{7,6},{8,9},{9,8},{10,11... | collective-permute-start | bytes 3145736 | tf_op jit(solution)/shard_map/ppermute | solution.py:310
  129.3 9.4 %all-to-all-start.3 = ((f32[8,3,256]{2,1,0:T(4,128)}), f32[8,3,256]{2,1,0:T(4,128)S(1)}, u32[]{:S(2)}, u32[]{:S(2)}) async-start(f32[8,3,256]{2,1,0:T(4,128)} %get-tuple-element.20), calls=%async_computation.3 | async-start | bytes 65536 | tf_op jit(solution)/shard_map/all_to_all | solution.py:308
Sparse Core Ops, SparseCore 0:
  33.4 78.1 all-gather.3
